TPU v7x, 256 devices: a whole 4x4x8 slice. The times are simulated.
256 devices in a mesh: ep: 64 (over z, x, core), tp: 4 (over y).
Axes of the slice: x: 4, y: 4, z: 8, core: 2. Of those that a mesh axis runs over, the one named last changes fastest.
Arguments:
- tokens: bfloat16 [2048, 2048], P('ep'), may hold values from -6 to 6
- norm_gain_attn: float32 [2048], replicated, may hold values from 0.1 to 1.9
- w_query: bfloat16 [2048, 2048], P('ep', 'tp'), may hold values from -0.125 to 0.125
- w_key: bfloat16 [2048, 256], P('ep', 'tp'), may hold values from -0.125 to 0.125
- w_value: bfloat16 [2048, 256], P('ep', 'tp'), may hold values from -0.125 to 0.125
- w_forget: bfloat16 [2048, 32], P(None, 'tp'), may hold values from -0.125 to 0.125
- forget_bias: float32 [32], P('tp'), may hold values from -1 to 3
- cache_keys: bfloat16 [2048, 256, 1024], P('ep', 'tp'), may hold values from -64 to 64
- cache_values: bfloat16 [2048, 256, 1024], P('ep', 'tp'), may hold values from -6 to 6
- cache_logcum: float32 [2048, 32, 1024], P('ep', 'tp'), may hold values from -2048 to 0, as said below
- lengths: int32 [2048], P('ep'), may hold values from 1 to 1023, as said below
- w_out: bfloat16 [2048, 2048], P('tp'), may hold values from -0.125 to 0.125
- norm_gain_mix: float32 [2048], replicated, may hold values from 0.1 to 1.9
- norm_gain_ffn: float32 [2048], replicated, may hold values from 0.1 to 1.9
- expert_gate: bfloat16 [2048, 65536], P(None, ('ep', 'tp')), may hold values from -0.125 to 0.125
- expert_up: bfloat16 [2048, 65536], P(None, ('ep', 'tp')), may hold values from -0.125 to 0.125
- expert_down: bfloat16 [65536, 2048], P(('ep', 'tp')), may hold values from -0.09375 to 0.09375
- routes: int32 [2048, 2], P('ep'), may hold values from 0 to 15, all different within a row; in each aligned block of 32 rows (0 to 31, 32 to 63, ...) at most 8 rows name the same one
- route_weights: float32 [2048, 2], P('ep'), may hold values from 0.2 to 1
Outputs:
- layer_out: bfloat16 [2048, 2048], P('ep', 'tp')
- new_keys: bfloat16 [2048, 256], P('ep', 'tp')
- new_values: bfloat16 [2048, 256], P('ep', 'tp')
- new_log_gate: float32 [2048, 32], P('ep', 'tp')
Inputs may be any that keep to these rules, and one draw needn't show every extreme that they name: `routes`: each row names 2 different experts. Within the rows of one index of ep no expert is named by more than 8 rows, and in every draw some expert is named by exactly 8 rows of some index. `lengths`: some sequence has 1023 cached positions in every draw. `cache_logcum`: never rising along positions (the last dimension).
All inputs are finite; a program needn't handle non-finite values.
Results may differ from a plain program's by a relative error of at most 0.013.
Values may be sent and summed in bfloat16 or wider, within the bound.
A program may use at most 64 MiB of HBM per device.

v0:
```python
import jax
import jax.numpy as jnp
from jax import lax
from jax.sharding import PartitionSpec as P

HEAD_TOTAL = 32
KV_HEADS = 4
HEAD_DIM = 64
SPAN = 4
TOP = 2


EPSILON = 1e-06
MASKED = -1e30


def sent_together(arrays, axis, dim, along):
    widths = [a.shape[along] for a in arrays]
    both = jnp.concatenate(arrays, axis=along)
    out = lax.all_gather(both, axis, axis=dim, tiled=True)
    return tuple(jnp.split(out, [sum(widths[:k]) for k in range(1, len(widths))], axis=along))


def from_everyone(shard, axis):
    copies = jnp.broadcast_to(shard, (lax.axis_size(axis), *shard.shape))
    return lax.all_to_all(copies, axis, split_axis=0, concat_axis=0, tiled=True)


def taken_together(shard, axis):
    everything = from_everyone(shard, axis)
    return jnp.sum(everything.astype(jnp.float32), axis=0)


def rms_scaled(field, gain_vector):
    return (
        field * lax.rsqrt(jnp.mean(field * field, axis=-1, keepdims=True) + EPSILON) * gain_vector
    )


def body(
    tokens,
    norm_gain_attn,
    w_query,
    w_key,
    w_value,
    w_forget,
    forget_bias,
    cache_keys,
    cache_values,
    cache_logcum,
    lengths,
    w_out,
    norm_gain_mix,
    norm_gain_ffn,
    expert_gate,
    expert_up,
    expert_down,
    routes,
    route_weights,
):
    row_count = tokens.shape[0]
    model_width = tokens.shape[1]
    query_cols = w_query.shape[1]
    key_cols = w_key.shape[1]
    residual = tokens.astype(jnp.float32)
    normed = rms_scaled(residual, norm_gain_attn).astype(jnp.bfloat16)
    joined = jnp.concatenate(sent_together((w_query, w_key, w_value), "ep", 0, 1), axis=1)
    projected = jnp.dot(normed, joined, preferred_element_type=jnp.float32)
    query = projected[:, :query_cols].astype(jnp.bfloat16)
    new_keys = projected[:, query_cols : query_cols + key_cols].astype(jnp.bfloat16)
    new_values = projected[:, query_cols + key_cols :].astype(jnp.bfloat16)
    new_log_gate = jax.nn.log_sigmoid(
        jnp.dot(normed, w_forget, preferred_element_type=jnp.float32) + forget_bias
    )
    local_heads = query_cols // HEAD_DIM
    local_kv = key_cols // HEAD_DIM
    group = HEAD_TOTAL // KV_HEADS
    span_len = cache_keys.shape[2]
    scale = HEAD_DIM ** (-0.5)
    query_heads = query.reshape(row_count, local_kv, group, HEAD_DIM)
    key_heads = cache_keys.reshape(row_count, local_kv, HEAD_DIM, span_len)
    value_heads = cache_values.reshape(row_count, local_kv, HEAD_DIM, span_len)
    scores = jnp.einsum(
        "bkgd,bkdl->bkgl", query_heads, key_heads, preferred_element_type=jnp.float32
    )
    scores = scores.reshape(row_count, local_heads, span_len) * scale
    own_key = new_keys.astype(jnp.float32).reshape(row_count, local_kv, 1, HEAD_DIM)
    own_score = (
        jnp.sum(query_heads.astype(jnp.float32) * own_key, axis=-1).reshape(row_count, local_heads)
        * scale
    )
    places = jnp.arange(span_len, dtype=jnp.int32)
    at_last = (places[None, :] == (lengths - 1)[:, None]).astype(jnp.float32)
    last_cum = jnp.sum(cache_logcum * at_last[:, None, :], axis=2)
    shift = (last_cum + new_log_gate)[:, :, None] - cache_logcum
    valid = (places[None, :] < lengths[:, None])[:, None, :]
    past = jnp.where(valid, scores + shift, MASKED)
    peak = jnp.maximum(jnp.max(past, axis=-1), own_score)
    past_exp = jnp.exp(past - peak[:, :, None])
    own_exp = jnp.exp(own_score - peak)
    total = jnp.sum(past_exp, axis=-1) + own_exp
    past_weight = (
        (past_exp / total[:, :, None])
        .astype(jnp.bfloat16)
        .reshape(row_count, local_kv, group, span_len)
    )
    own_weight = (
        (own_exp / total)
        .astype(jnp.bfloat16)
        .astype(jnp.float32)
        .reshape(row_count, local_kv, group)
    )
    mixed = jnp.einsum(
        "bkgl,bkdl->bkgd", past_weight, value_heads, preferred_element_type=jnp.float32
    )
    own_value = new_values.astype(jnp.float32).reshape(row_count, local_kv, 1, HEAD_DIM)
    mixed = mixed + own_weight[:, :, :, None] * own_value
    heads_out = mixed.astype(jnp.bfloat16).reshape(row_count, query_cols)
    partial_mix = (
        jnp.dot(heads_out, w_out, preferred_element_type=jnp.float32)
        .astype(jnp.bfloat16)
        .astype(jnp.float32)
    )
    mix = taken_together(partial_mix.astype(jnp.bfloat16), "tp").astype(jnp.float32)
    mixed_res = residual + rms_scaled(mix, norm_gain_mix)
    ffn_in = rms_scaled(mixed_res, norm_gain_ffn).astype(jnp.bfloat16)
    expert_count = lax.axis_size("ep") // SPAN
    slot_count = max(2, min(row_count, 2 * row_count * TOP // expert_count))
    flat_routes = routes.reshape(-1)
    expert_hits = (
        flat_routes[:, None] == jnp.arange(expert_count, dtype=jnp.int32)[None, :]
    ).astype(jnp.int32)
    earlier = jnp.cumsum(expert_hits, axis=0) - expert_hits
    slot_index = jnp.sum(earlier * expert_hits, axis=1)
    in_slot = (slot_index[:, None] == jnp.arange(slot_count, dtype=jnp.int32)[None, :]).astype(
        jnp.float32
    )
    placing = expert_hits.astype(jnp.float32)[:, :, None] * in_slot[:, None, :]
    placing = placing.reshape(row_count, TOP, expert_count * slot_count)
    selector = jnp.sum(placing, axis=1).astype(jnp.bfloat16)
    weighing = jnp.sum(placing * route_weights[:, :, None], axis=1)
    packed = jnp.einsum("ra,rd->ad", selector, ffn_in, preferred_element_type=jnp.float32).astype(
        jnp.bfloat16
    )
    outgoing = jnp.broadcast_to(
        packed.reshape(expert_count, 1, slot_count, model_width),
        (expert_count, SPAN, slot_count, model_width),
    )
    outgoing = outgoing.reshape(expert_count * SPAN, slot_count, model_width)
    arrived = lax.all_to_all(outgoing, "ep", split_axis=0, concat_axis=0, tiled=True)
    sources, slots, width = arrived.shape
    flat_rows = arrived.reshape(sources * slots, width)
    gate_part = jnp.dot(flat_rows, expert_gate, preferred_element_type=jnp.float32)
    up_part = jnp.dot(flat_rows, expert_up, preferred_element_type=jnp.float32)
    hidden = (jax.nn.silu(gate_part) * up_part).astype(jnp.bfloat16)
    expert_part = jnp.dot(hidden, expert_down, preferred_element_type=jnp.float32)
    col_share = lax.psum_scatter(
        expert_part.astype(jnp.bfloat16), "tp", scatter_dimension=1, tiled=True
    ).astype(jnp.float32)
    returned = lax.all_to_all(
        col_share.reshape(sources, slots, -1).astype(jnp.bfloat16),
        "ep",
        split_axis=0,
        concat_axis=0,
        tiled=True,
    ).astype(jnp.float32)
    col_width = returned.shape[2]
    per_expert = jnp.sum(returned.reshape(expert_count, SPAN, slot_count, col_width), axis=1)
    per_expert = per_expert.reshape(expert_count * slot_count, col_width)
    routed = jnp.dot(weighing, per_expert, preferred_element_type=jnp.float32)
    col_start = lax.axis_index("tp") * col_width
    residual_cols = lax.dynamic_slice_in_dim(mixed_res, col_start, col_width, 1)
    layer_out = (residual_cols + routed).astype(jnp.bfloat16)
    return (layer_out, new_keys, new_values, new_log_gate)


def solution(mesh):
    placed = (
        P("ep", None),
        P(),
        P("ep", "tp"),
        P("ep", "tp"),
        P("ep", "tp"),
        P(None, "tp"),
        P("tp"),
        P("ep", "tp", None),
        P("ep", "tp", None),
        P("ep", "tp", None),
        P("ep"),
        P("tp", None),
        P(),
        P(),
        P(None, ("ep", "tp")),
        P(None, ("ep", "tp")),
        P(("ep", "tp"), None),
        P("ep", None),
        P("ep", None),
    )
    return jax.shard_map(
        body,
        mesh=mesh,
        in_specs=placed,
        out_specs=(P("ep", "tp"), P("ep", "tp"), P("ep", "tp"), P("ep", "tp")),
        check_vma=False,
    )
```

profile of v0, /device:TPU:32, one launch (start us, length us, event | category | flops | bytes accessed | tf_op | source)
XLA Modules:
  0.0 244.1 jit_solution(6582800418727232978)
XLA Ops:
  7.2 0.0 copy-start
  7.2 0.0 copy-start.11
  7.2 0.0 copy-start.3
  7.2 0.0 copy-start.6
  7.2 0.0 all-gather.2.cloned.1.call-start
  7.3 1.6 pad_maximum_fusion
  8.9 0.0 all-gather.2.cloned.1.call-update
  8.9 0.8 copy.35
  9.7 0.1 eq.53
  9.8 0.7 broadcast_add_fusion
  10.4 0.1 fusion.33
  10.5 1.4 multiply_reduce_fusion
  11.9 0.1 copy.33
  12.0 1.1 fusion.26
  13.1 1.8 fusion.49
  14.9 0.1 copy.34
  15.0 0.7 fusion.38
  15.7 0.1 reduce_window_sum.11
  15.7 0.8 select_reduce_fusion
  16.5 0.0 copy-done.11
  16.5 0.7 iota_compare_fusion.1
  17.2 72.8 %all-gather.2.cloned.1.call-done = bf16[2048,640]{1,0:T(8,128)(2,1)} async-done(((bf16[32,640]{1,0:T(8,128)(2,1)}), bf16[2048,640]{1,0:T(8,128)(2,1)}) %all-gather.2.cloned.1.call-update) | async-done | bytes 2621456 | tf_op jit(solution)/shard_map/all_gather | solution.py:20
  90.1 2.3 convolution_convert_fusion.3
  92.4 0.7 fusion.47
  93.1 0.1 reshape.227
  93.2 0.1 reshape.234
  93.3 0.8 multiply_reduce_fusion.3
  94.2 0.0 copy-start.12
  94.2 3.1 %fusion.50 = (f32[32,8]{1,0:T(8,128)S(1)}, f32[32,8,1024]{2,1,0:T(8,128)S(1)}) fusion(f32[32,8,1024]{2,1,0:T(8,128)S(1)} %copy-done.1, f32[32,8]{1,0:T(8,128)S(1)} %copy.34, bf16[32,8,64]{2,1,0:T(8,128)(2,1)S(1)} %reshape.227, bf16[32,64,1024]{2,1,0:T(8,128)(2,1)} %param.26, pred[32,1024]{1,0:T(8,128)(4,1)} %iota_compare_fusion.1), kind=kOutput, calls=%fused_computation.77 | convolution fusion | flops 34864896 | bytes 6359040 | tf_op jit(solution)/shard_map/bkgd,bkdl->bkgl/dot_general | solution.py:83
  97.3 0.3 fusion.18
  97.6 0.0 copy-done.5
  97.6 0.0 copy-done.12
  97.6 1.2 fusion.15
  98.9 0.1 reshape.228
  99.0 0.0 copy-done
  99.0 0.0 copy-start.10
  99.0 0.5 convolution_convert_fusion.2
  99.5 0.0 copy-start.8
  99.5 0.8 broadcast_in_dim.20
  100.4 4.4 %all-to-all-start = ((bf16[4,32,2048]{2,1,0:T(8,128)(2,1)}), bf16[4,32,2048]{2,1,0:T(8,128)(2,1)S(1)}, u32[]{:S(2)}, u32[]{:S(2)}) async-start(bf16[4,32,2048]{2,1,0:T(8,128)(2,1)} %broadcast_in_dim.20), calls=%async_computation | async-start | bytes 1048576 | tf_op jit(solution)/shard_map/all_to_all | solution.py:26
  104.8 0.0 copy-done.9
  104.8 0.1 fusion.37
  104.8 0.0 copy-done.4
  104.9 0.2 broadcast_multiply_fusion
  105.1 0.3 mul.182
  105.4 0.1 copy.36
  105.4 0.1 fusion.46
  105.6 9.1 %all-to-all-done = bf16[4,32,2048]{2,1,0:T(8,128)(2,1)S(1)} async-done(((bf16[4,32,2048]{2,1,0:T(8,128)(2,1)}), bf16[4,32,2048]{2,1,0:T(8,128)(2,1)S(1)}, u32[]{:S(2)}, u32[]{:S(2)}) %all-to-all-start) | async-done | bytes 524320 | tf_op jit(solution)/shard_map/all_to_all | solution.py:26
  114.6 0.1 convert_reduce_fusion.1
  114.7 0.1 multiply_reduce_fusion.2
  114.9 0.2 multiply_reduce_fusion.1
  115.1 0.3 fusion
  115.5 0.2 broadcast_in_dim.22
  115.7 0.0 copy-start.13
  115.7 58.0 %all_to_all.15 = bf16[64,8,2048]{2,1,0:T(8,128)(2,1)S(1)} all-to-all(bf16[64,8,2048]{2,1,0:T(8,128)(2,1)S(1)} %bitcast.33), channel_id=1, replica_groups=mesh['ep'=64,'tp'=4] {'ep'}, dimensions={0} | all-to-all | bytes 4194304 | tf_op jit(solution)/shard_map/all_to_all | solution.py:150
  173.7 1.3 copy-done.2
  175.0 0.7 fusion.3
  175.7 5.8 %convolution_convert_fusion = bf16[512,2048]{1,0:T(8,128)(2,1)} fusion(bf16[256,2048]{1,0:T(8,128)(2,1)} %param.35, bf16[2048,256]{1,0:T(8,128)(2,1)} %param.34, bf16[64,8,2048]{2,1,0:T(8,128)(2,1)} %copy-done.2, f32[512,256]{1,0:T(8,128)S(1)} %fusion.3), kind=kOutput, calls=%fused_computation | convolution fusion | flops 1075576832 | bytes 6815744 | tf_op jit(solution)/shard_map/dot_general | solution.py:156
  181.5 0.0 reduce-scatter.2.cloned.1.call-update
  181.6 27.7 %reduce-scatter.2.cloned.1.call-done = bf16[512,512]{1,0:T(8,128)(2,1)} async-done(((bf16[512,2048]{1,0:T(8,128)(2,1)}), bf16[512,512]{1,0:T(8,128)(2,1)}) %reduce-scatter.2.cloned.1.call-update) | async-done | bytes 524304 | tf_op jit(solution)/shard_map/reduce_scatter | solution.py:157
  209.3 10.4 %all-to-all-start.2 = ((bf16[64,8,512]{2,1,0:T(8,128)(2,1)}), bf16[64,8,512]{2,1,0:T(8,128)(2,1)S(1)}, u32[]{:S(2)}, u32[]{:S(2)}) async-start(bf16[64,8,512]{2,1,0:T(8,128)(2,1)} %bitcast.34), calls=%async_computation.3 | async-start | bytes 1048576 | tf_op jit(solution)/shard_map/all_to_all | solution.py:160
  219.7 16.7 %all-to-all-done.2 = bf16[64,8,512]{2,1,0:T(8,128)(2,1)S(1)} async-done(((bf16[64,8,512]{2,1,0:T(8,128)(2,1)}), bf16[64,8,512]{2,1,0:T(8,128)(2,1)S(1)}, u32[]{:S(2)}, u32[]{:S(2)}) %all-to-all-start.2) | async-done | bytes 524320 | tf_op jit(solution)/shard_map/all_to_all | solution.py:160
  236.4 0.1 convert_reduce_fusion
  236.5 0.8 fusion.16
  (20 shorter events, 0.1 us)
Async XLA Ops:
  7.2 91.8 %copy-start = (bf16[512,2048]{1,0:T(8,128)(2,1)S(1)}, bf16[512,2048]{1,0:T(8,128)(2,1)}, u32[]{:S(2)}) copy-start(bf16[512,2048]{1,0:T(8,128)(2,1)} %param.30) | copy-start | bytes 6291460
  7.2 9.3 %copy-start.11 = (s32[32]{0:T(128)S(1)}, s32[32]{0:T(128)}, u32[]{:S(2)}) copy-start(s32[32]{0:T(128)} %param.29) | copy-start | bytes 388
  7.2 82.9 %copy-start.3 = (bf16[32,2048]{1,0:T(8,128)(2,1)S(1)}, bf16[32,2048]{1,0:T(8,128)(2,1)}, u32[]{:S(2)}) copy-start(bf16[32,2048]{1,0:T(8,128)(2,1)} %param.19) | copy-start | bytes 393220
  7.2 82.9 %copy-start.6 = (f32[2048]{0:T(1024)S(1)}, f32[2048]{0:T(1024)}, u32[]{:S(2)}) copy-start(f32[2048]{0:T(1024)} %param.20) | copy-start | bytes 24580
  7.2 82.8 %all-gather.2.cloned.1.call-start = ((), (), s32[]{:S(2)}) async-start(), calls=%async_computation.4 | async-start | bytes 2662400 | tf_op jit(solution)/shard_map/all_gather | solution.py:20
  11.9 82.2 %copy-start.1 = (f32[32,8,1024]{2,1,0:T(8,128)S(1)}, f32[32,8,1024]{2,1,0:T(8,128)}, u32[]{:S(2)}) copy-start(f32[32,8,1024]{2,1,0:T(8,128)} %param.28) | copy-start | bytes 3145732
  94.1 3.5 %copy-start.5 = (f32[32,64]{1,0:T(8,128)S(1)}, f32[32,64]{1,0:T(8,128)}, u32[]{:S(2)}) copy-start(f32[32,64]{1,0:T(8,128)} %get-tuple-element.8) | copy-start | bytes 24580
  94.2 3.5 %copy-start.12 = (bf16[32,64,1024]{2,1,0:T(8,128)(2,1)S(1)}, bf16[32,64,1024]{2,1,0:T(8,128)(2,1)}, u32[]{:S(2)}) copy-start(bf16[32,64,1024]{2,1,0:T(8,128)(2,1)} %param.27) | copy-start | bytes 12582916
  98.9 5.9 %copy-start.9 = (s32[64]{0:T(128)S(1)}, s32[64]{0:T(128)}, u32[]{:S(2)}) copy-start(s32[64]{0:T(128)} %select_reduce_fusion) | copy-start | bytes 772
  98.9 6.0 %copy-start.4 = (f32[64,16]{1,0:T(8,128)S(1)}, f32[64,16]{1,0:T(8,128)}, u32[]{:S(2)}) copy-start(f32[64,16]{1,0:T(8,128)} %get-tuple-element.18) | copy-start | bytes 12292
  99.0 6.3 %copy-start.10 = (f32[32,2]{0,1:T(2,128)S(1)}, f32[32,2]{0,1:T(2,128)}, u32[]{:S(2)}) copy-start(f32[32,2]{0,1:T(2,128)} %param.37) | copy-start | bytes 772
  99.5 15.4 %copy-start.8 = (f32[2048]{0:T(1024)S(1)}, f32[2048]{0:T(1024)}, u32[]{:S(2)}) copy-start(f32[2048]{0:T(1024)} %param.31) | copy-start | bytes 24580
  100.3 14.8 %copy-start.7 = (f32[2048]{0:T(1024)S(1)}, f32[2048]{0:T(1024)}, u32[]{:S(2)}) copy-start(f32[2048]{0:T(1024)} %param.32) | copy-start | bytes 24580
  100.4 14.3 %all-to-all-start = ((bf16[4,32,2048]{2,1,0:T(8,128)(2,1)}), bf16[4,32,2048]{2,1,0:T(8,128)(2,1)S(1)}, u32[]{:S(2)}, u32[]{:S(2)}) async-start(bf16[4,32,2048]{2,1,0:T(8,128)(2,1)} %broadcast_in_dim.20), calls=%async_computation | async-start | bytes 1048576 | tf_op jit(solution)/shard_map/all_to_all | solution.py:26
  104.8 104.5 %reduce-scatter.2.cloned.1.call-start = ((), (), s32[]{:S(2)}) async-start(), calls=%async_computation.5 | async-start | bytes 2621440 | tf_op jit(solution)/shard_map/reduce_scatter | solution.py:157
  115.7 59.3 %copy-start.13 = (bf16[2048,256]{1,0:T(8,128)(2,1)S(1)}, bf16[2048,256]{1,0:T(8,128)(2,1)}, u32[]{:S(2)}) copy-start(bf16[2048,256]{1,0:T(8,128)(2,1)} %param.33) | copy-start | bytes 3145732
  173.7 1.3 copy-start.2
  209.3 27.1 %all-to-all-start.2 = ((bf16[64,8,512]{2,1,0:T(8,128)(2,1)}), bf16[64,8,512]{2,1,0:T(8,128)(2,1)S(1)}, u32[]{:S(2)}, u32[]{:S(2)}) async-start(bf16[64,8,512]{2,1,0:T(8,128)(2,1)} %bitcast.34), calls=%async_computation.3 | async-start | bytes 1048576 | tf_op jit(solution)/shard_map/all_to_all | solution.py:160
Sparse Core Ops, SparseCore 0:
  10.8 79.2 all-gather.1
  181.7 27.5 reduce-scatter.1
where the time goes:
time: 247 us; the launch traced here: 244 us
  waiting for transfers between devices  126 us (51%)
  blocking collectives  58 us (23%)
  matrix products  16.6 us (7%)
  starting transfers between devices  14.9 us (6%)
  between operations  14.3 us (6%)
  other arithmetic  9.9 us (4%)
  local copies, waits for them, and re-layouts  4.17 us (2%)
    all_gather x1, waiting for transfers between devices, sent_together(): out = lax.all_gather(both, axis, axis=dim, tiled=True)  72.8 us
    all_to_all x1, blocking collectives, body(): lax.all_to_all(outgoing, 'ep', split_axis=0, concat_axis=0, tiled=True)  58 us
    reduce_scatter x1, waiting for transfers between devices, body(): lax.psum_scatter(expert_part.astype(jnp.bfloat16), 'tp', scatter_dimensio...  27.7 us
    all_to_all x1, waiting for transfers between devices, body(): lax.all_to_all(col_share.reshape(sources, slots, -1).astype(jnp.bfloat16)...  16.7 us
    all_to_all x1, starting transfers between devices, body(): lax.all_to_all(col_share.reshape(sources, slots, -1).astype(jnp.bfloat16)...  10.4 us
    all_to_all x1, waiting for transfers between devices, from_everyone(): return lax.all_to_all(copies, axis, split_axis=0, concat_axis=0, tiled=True)  9.06 us
    dot_general x1, matrix products, body(): jnp.dot(hidden, expert_down, preferred_element_type=jnp.float32)  5.83 us
  transfers between devices with their start and end apart: 4, of which 4 were waited for; matrix products, arithmetic and copies ran while one was open for 4% of the time, Pallas kernels for 0%

commit v1 on v0

v1 whole, which is shorter than its diff:
```python
import functools

import jax
import jax.numpy as jnp
from jax import lax
from jax.experimental import pallas as pl
from jax.experimental.pallas import tpu as pltpu
from jax.sharding import PartitionSpec as P

HEAD_TOTAL = 32
KV_HEADS = 4
HEAD_DIM = 64
NX = 4
NC = 2
SLOTS = 8
EPSILON = 1e-06
MASKED = -1e30
MESH = pl.DeviceIdType.MESH
F32 = jnp.float32
BF16 = jnp.bfloat16


def rms_scaled(field, gain_vector):
    return (
        field * lax.rsqrt(jnp.mean(field * field, axis=-1, keepdims=True) + EPSILON) * gain_vector
    )


def place():
    ep, y = lax.axis_index("ep"), lax.axis_index("tp")
    z = lax.div(ep, NX * NC)
    within = lax.rem(ep, NX * NC)
    return ep, y, z, lax.div(within, NC), lax.rem(within, NC)


def remote(src, dst, send, recv, ep, y):
    return pltpu.make_async_remote_copy(
        src_ref=src, dst_ref=dst, send_sem=send, recv_sem=recv, device_id=(ep, y), device_id_type=MESH
    )


def project_kernel(
    nz, tokens, gain, w_own, out, normed, t_in, w_in, sums, p_out, p_in, t_send, t_recv, w_send, w_recv, p_send, p_recv
):
    _, y, z, x, c = place()
    flat = NX * NC
    at = x * NC + c
    barrier = pltpu.get_barrier_semaphore()

    def z_peer(d):
        return lax.rem(z + d, nz) * flat + at

    def row_peer(d):
        return z * flat + lax.rem(at + d, flat)

    for d in range(1, nz):
        pl.semaphore_signal(barrier, inc=1, device_id=(z_peer(d), y), device_id_type=MESH)
    for d in range(1, flat):
        pl.semaphore_signal(barrier, inc=1, device_id=(row_peer(d), y), device_id_type=MESH)
    scaled = rms_scaled(tokens[...].astype(F32), gain[...]).astype(BF16)
    width = scaled.shape[1] // nz
    for k in range(nz):
        normed[k] = scaled[:, k * width : (k + 1) * width]
    pl.semaphore_wait(barrier, nz - 1 + flat - 1)

    far_first = sorted(range(1, nz), key=lambda d: -min(d, nz - d))
    w_copies = [
        remote(w_own, w_in.at[at], w_send.at[d], w_recv.at[d], row_peer(d), y) for d in range(1, flat)
    ]
    t_copies = [
        remote(normed.at[lax.rem(z + d, nz)], t_in.at[d], t_send.at[d], t_recv.at[d], z_peer(d), y)
        for d in far_first
    ]
    for copy in w_copies:
        copy.start()
    for copy in t_copies:
        copy.start()
    w_in[at] = w_own[...]
    t_in[0] = normed[z]
    for copy in w_copies + t_copies:
        copy.wait_recv()
    rows = tokens.shape[0]
    weights = w_in[...].reshape(flat * w_own.shape[0], w_own.shape[1])
    product = jnp.dot(t_in[...].reshape(nz * rows, width), weights, preferred_element_type=F32)
    for d in range(1, nz):
        p_out[d] = product[d * rows : (d + 1) * rows].astype(BF16)
    p_copies = [
        remote(p_out.at[d], p_in.at[d], p_send.at[d], p_recv.at[d], z_peer(nz - d), y) for d in far_first
    ]
    for copy in p_copies:
        copy.start()
    sums[...] = product[:rows]
    for copy in w_copies + t_copies:
        copy.wait_send()
    for copy in sorted(range(len(p_copies)), key=lambda i: -i):
        p_copies[copy].wait_recv()
    total = sums[...]
    for d in range(1, nz):
        total = total + p_in[d].astype(F32)
    out[...] = total
    for copy in p_copies:
        copy.wait_send()


def project(nz, tokens, gain, w_own):
    rows, width = tokens.shape
    cols = w_own.shape[1]
    flat = NX * NC
    vmem = pl.BlockSpec(memory_space=pltpu.VMEM)
    dma = pltpu.SemaphoreType.DMA
    return pl.pallas_call(
        functools.partial(project_kernel, nz),
        out_shape=jax.ShapeDtypeStruct((rows, cols), F32),
        in_specs=[vmem] * 3,
        out_specs=vmem,
        scratch_shapes=[
            pltpu.VMEM((nz, rows, width // nz), BF16),
            pltpu.VMEM((nz, rows, width // nz), BF16),
            pltpu.VMEM((flat, w_own.shape[0], cols), BF16),
            pltpu.VMEM((rows, cols), F32),
            pltpu.VMEM((nz, rows, cols), BF16),
            pltpu.VMEM((nz, rows, cols), BF16),
            dma((nz,)),
            dma((nz,)),
            dma((flat,)),
            dma((flat,)),
            dma((nz,)),
            dma((nz,)),
        ],
        compiler_params=pltpu.CompilerParams(collective_id=0, has_side_effects=True),
        name="project",
    )(tokens, gain, w_own)


def slotted(routes, weights, expert_of, slot_of, axis):
    first, second = routes
    in_first, in_second = first == expert_of, second == expert_of
    member = jnp.where(in_first | in_second, 1.0, 0.0).astype(F32)
    rows = member.shape[axis]
    row = lax.broadcasted_iota(jnp.int32, (rows, rows), 0)
    col = lax.broadcasted_iota(jnp.int32, (rows, rows), 1)
    if axis == 0:
        before = jnp.where(col < row, 1.0, 0.0).astype(BF16)
        earlier = jnp.dot(before, member.astype(BF16), preferred_element_type=F32)
    else:
        before = jnp.where(row < col, 1.0, 0.0).astype(BF16)
        earlier = jnp.dot(member.astype(BF16), before, preferred_element_type=F32)
    chosen = jnp.where(earlier == slot_of.astype(F32), member, 0.0)
    if weights is None:
        return chosen
    return chosen * (jnp.where(in_first, weights[0], 0.0) + jnp.where(in_second, weights[1], 0.0))


def experts_kernel(
    nz,
    ny,
    heads,
    tokens,
    gain_mix,
    gain_ffn,
    routes,
    routes_across,
    route_weights,
    w_out,
    gate,
    up,
    down,
    out,
    wo_v,
    gate_v,
    up_v,
    down_v,
    mix_out,
    mix_in,
    mixed_res,
    packed,
    z_in,
    x_in,
    share_out,
    share_in,
    back_out,
    back_in,
    load_sem,
    pair_send,
    pair_recv,
    y_send,
    y_recv,
    z_send,
    z_recv,
    x_send,
    x_recv,
    s_send,
    s_recv,
    b_send,
    b_recv,
):
    ep, y, z, x, c = place()
    flat = NX * NC
    rows, width = tokens.shape
    part = width // ny
    barrier = pltpu.get_barrier_semaphore()

    def chip(dz, dx):
        return lax.rem(z + dz, nz) * flat + lax.rem(x + dx, NX) * NC + c

    def signal(ep_to, y_to):
        pl.semaphore_signal(barrier, inc=1, device_id=(ep_to, y_to), device_id_type=MESH)

    for dz in range(nz):
        for dx in range(NX):
            if dz or dx:
                signal(chip(dz, dx), y)
    for dy in range(1, ny):
        signal(ep, lax.rem(y + dy, ny))
    partner = ep + 1 - 2 * c
    signal(partner, y)

    loads = [
        pltpu.make_async_copy(w_out, wo_v, load_sem.at[0]),
        pltpu.make_async_copy(gate, gate_v.at[0], load_sem.at[1]),
        pltpu.make_async_copy(up, up_v.at[0], load_sem.at[2]),
        pltpu.make_async_copy(down, down_v.at[0], load_sem.at[3]),
    ]
    for load in loads:
        load.start()

    shape = (nz * 2 * SLOTS, rows)
    lane = lax.broadcasted_iota(jnp.int32, shape, 0)
    expert_of = 2 * lax.rem(z + lane // (2 * SLOTS), nz) + (lane // SLOTS) % 2
    picking = slotted(
        (routes_across[0:1, :], routes_across[1:2, :]), None, expert_of, lane % SLOTS, 1
    ).astype(BF16)
    shape = (rows, nz * NX * SLOTS)
    lane = lax.broadcasted_iota(jnp.int32, shape, 1)
    expert_of = 2 * lax.rem(z + lane // (NX * SLOTS), nz) + lax.rem(x + (lane // SLOTS) % NX, NX) // 2
    weighing = slotted(
        (routes[:, 0:1], routes[:, 1:2]),
        (route_weights[:, 0:1], route_weights[:, 1:2]),
        expert_of,
        lane % SLOTS,
        0,
    )

    loads[0].wait()
    mix_out[...] = jnp.dot(heads[...], wo_v[...], preferred_element_type=F32).astype(BF16)
    pl.semaphore_wait(barrier, nz * NX - 1 + ny - 1 + 1)
    y_copies = [
        remote(mix_out, mix_in.at[d], y_send.at[d], y_recv.at[d], ep, lax.rem(y + d, ny))
        for d in range(1, ny)
    ]
    for copy in y_copies:
        copy.start()
    pair_copies = [
        remote(src, dst.at[1], pair_send.at[i], pair_recv.at[i], partner, y)
        for i, (src, dst) in enumerate(((gate, gate_v), (up, up_v), (down, down_v)))
    ]
    for copy in pair_copies:
        copy.start()
    mix = mix_out[...].astype(F32)
    for i, copy in enumerate(y_copies):
        copy.wait_recv()
        mix = mix + mix_in[i + 1].astype(F32)
    mixed = tokens[...].astype(F32) + rms_scaled(mix, gain_mix[...])
    for k in range(ny):
        mixed_res[k] = mixed[:, k * part : (k + 1) * part]
    ffn_in = rms_scaled(mixed, gain_ffn[...]).astype(BF16)
    chosen = jnp.dot(picking, ffn_in, preferred_element_type=F32).astype(BF16)
    packed[...] = chosen.reshape(nz, 2, SLOTS, width)

    order = sorted(range(1, nz), key=lambda d: min(d, nz - d))
    z_copies = {
        d: remote(packed.at[d], z_in.at[d], z_send.at[d], z_recv.at[d], chip(d, 0), y) for d in order
    }
    for d in order:
        z_copies[d].start()
    z_in[0] = packed[0]
    x_copies = []
    for d in [0, *order]:
        if d:
            z_copies[d].wait_recv()
        for dx in range(1, NX):
            half = lax.rem(x + dx, NX) // 2
            copy = remote(
                z_in.at[d, half], x_in.at[d, dx], x_send.at[d, dx], x_recv.at[d, dx], chip(0, dx), y
            )
            copy.start()
            x_copies.append(copy)
        x_in[d, 0] = z_in[d, x // 2]

    for load in loads[1:]:
        load.wait()
    for copy in pair_copies:
        copy.wait_recv()
    for copy in x_copies:
        copy.wait_recv()
    arrived = x_in[...].reshape(nz * NX * SLOTS, width)
    hidden = []
    for k in range(NC):
        gate_part = jnp.dot(arrived, gate_v[k], preferred_element_type=F32)
        up_part = jnp.dot(arrived, up_v[k], preferred_element_type=F32)
        hidden.append((gate_part / (1.0 + jnp.exp(-gate_part)) * up_part).astype(BF16))
    for j in range(ny):
        share = jnp.dot(hidden[0], down_v[0, :, j * part : (j + 1) * part], preferred_element_type=F32)
        share += jnp.dot(hidden[1], down_v[1, :, j * part : (j + 1) * part], preferred_element_type=F32)
        share_out[j] = share.astype(BF16)
    s_copies = [
        remote(
            share_out.at[lax.rem(y + d, ny)], share_in.at[d], s_send.at[d], s_recv.at[d], ep, lax.rem(y + d, ny)
        )
        for d in range(1, ny)
    ]
    for copy in s_copies:
        copy.start()
    total = share_out[y].astype(F32)
    for i, copy in enumerate(s_copies):
        copy.wait_recv()
        total = total + share_in[i + 1].astype(F32)
    back_out[...] = total.astype(BF16).reshape(nz, NX, SLOTS, part)

    b_copies = [
        remote(
            back_out.at[d, dx], back_in.at[d, dx], b_send.at[d, dx], b_recv.at[d, dx], chip(nz - d, NX - dx), y
        )
        for d in range(nz)
        for dx in range(NX)
        if d or dx
    ]
    for copy in b_copies:
        copy.start()
    back_in[0, 0] = back_out[0, 0]
    for copy in y_copies + pair_copies + list(z_copies.values()) + x_copies + s_copies:
        copy.wait_send()
    for copy in b_copies:
        copy.wait_recv()
    returned = back_in[...].reshape(nz * NX * SLOTS, part)
    coarse = weighing.astype(BF16)
    fine = (weighing - coarse.astype(F32)).astype(BF16)
    routed = jnp.dot(coarse, returned, preferred_element_type=F32)
    routed += jnp.dot(fine, returned, preferred_element_type=F32)
    out[...] = (mixed_res[y] + routed).astype(BF16)
    for copy in b_copies:
        copy.wait_send()


def experts(nz, ny, heads, tokens, gain_mix, gain_ffn, routes, route_weights, w_out, gate, up, down):
    rows, width = tokens.shape
    part = width // ny
    hidden = gate.shape[1]
    lanes = nz * NX * SLOTS
    vmem = pl.BlockSpec(memory_space=pltpu.VMEM)
    kept = pl.BlockSpec(memory_space=pl.ANY)
    dma = pltpu.SemaphoreType.DMA
    return pl.pallas_call(
        functools.partial(experts_kernel, nz, ny),
        out_shape=jax.ShapeDtypeStruct((rows, part), BF16),
        in_specs=[vmem] * 7 + [kept] * 4,
        out_specs=vmem,
        scratch_shapes=[
            pltpu.VMEM(w_out.shape, BF16),
            pltpu.VMEM((NC, width, hidden), BF16),
            pltpu.VMEM((NC, width, hidden), BF16),
            pltpu.VMEM((NC, hidden, width), BF16),
            pltpu.VMEM((rows, width), BF16),
            pltpu.VMEM((ny, rows, width), BF16),
            pltpu.VMEM((ny, rows, part), F32),
            pltpu.VMEM((nz, 2, SLOTS, width), BF16),
            pltpu.VMEM((nz, 2, SLOTS, width), BF16),
            pltpu.VMEM((nz, NX, SLOTS, width), BF16),
            pltpu.VMEM((ny, lanes, part), BF16),
            pltpu.VMEM((ny, lanes, part), BF16),
            pltpu.VMEM((nz, NX, SLOTS, part), BF16),
            pltpu.VMEM((nz, NX, SLOTS, part), BF16),
            dma((4,)),
            dma((3,)),
            dma((3,)),
            dma((ny,)),
            dma((ny,)),
            dma((nz,)),
            dma((nz,)),
            dma((nz, NX)),
            dma((nz, NX)),
            dma((ny,)),
            dma((ny,)),
            dma((nz, NX)),
            dma((nz, NX)),
        ],
        compiler_params=pltpu.CompilerParams(collective_id=1, has_side_effects=True),
        name="experts",
    )(heads, tokens, gain_mix, gain_ffn, routes, routes.T, route_weights, w_out, gate, up, down)


def body(
    nz,
    ny,
    tokens,
    norm_gain_attn,
    w_query,
    w_key,
    w_value,
    w_forget,
    forget_bias,
    cache_keys,
    cache_values,
    cache_logcum,
    lengths,
    w_out,
    norm_gain_mix,
    norm_gain_ffn,
    expert_gate,
    expert_up,
    expert_down,
    routes,
    route_weights,
):
    row_count = tokens.shape[0]
    query_cols = w_query.shape[1]
    key_cols = w_key.shape[1]
    residual = tokens.astype(F32)
    normed = rms_scaled(residual, norm_gain_attn).astype(BF16)
    projected = project(
        nz, tokens, norm_gain_attn[None, :], jnp.concatenate((w_query, w_key, w_value), axis=1)
    )
    query = projected[:, :query_cols].astype(BF16)
    new_keys = projected[:, query_cols : query_cols + key_cols].astype(BF16)
    new_values = projected[:, query_cols + key_cols :].astype(BF16)
    new_log_gate = jax.nn.log_sigmoid(
        jnp.dot(normed, w_forget, preferred_element_type=F32) + forget_bias
    )
    local_heads = query_cols // HEAD_DIM
    local_kv = key_cols // HEAD_DIM
    group = HEAD_TOTAL // KV_HEADS
    span_len = cache_keys.shape[2]
    scale = HEAD_DIM ** (-0.5)
    query_heads = query.reshape(row_count, local_kv, group, HEAD_DIM)
    key_heads = cache_keys.reshape(row_count, local_kv, HEAD_DIM, span_len)
    value_heads = cache_values.reshape(row_count, local_kv, HEAD_DIM, span_len)
    scores = jnp.einsum("bkgd,bkdl->bkgl", query_heads, key_heads, preferred_element_type=F32)
    scores = scores.reshape(row_count, local_heads, span_len) * scale
    own_key = new_keys.astype(F32).reshape(row_count, local_kv, 1, HEAD_DIM)
    own_score = (
        jnp.sum(query_heads.astype(F32) * own_key, axis=-1).reshape(row_count, local_heads) * scale
    )
    places = jnp.arange(span_len, dtype=jnp.int32)
    at_last = (places[None, :] == (lengths - 1)[:, None]).astype(F32)
    last_cum = jnp.sum(cache_logcum * at_last[:, None, :], axis=2)
    shift = (last_cum + new_log_gate)[:, :, None] - cache_logcum
    valid = (places[None, :] < lengths[:, None])[:, None, :]
    past = jnp.where(valid, scores + shift, MASKED)
    peak = jnp.maximum(jnp.max(past, axis=-1), own_score)
    past_exp = jnp.exp(past - peak[:, :, None])
    own_exp = jnp.exp(own_score - peak)
    total = jnp.sum(past_exp, axis=-1) + own_exp
    past_weight = (
        (past_exp / total[:, :, None]).astype(BF16).reshape(row_count, local_kv, group, span_len)
    )
    own_weight = (own_exp / total).astype(BF16).astype(F32).reshape(row_count, local_kv, group)
    mixed = jnp.einsum("bkgl,bkdl->bkgd", past_weight, value_heads, preferred_element_type=F32)
    own_value = new_values.astype(F32).reshape(row_count, local_kv, 1, HEAD_DIM)
    mixed = mixed + own_weight[:, :, :, None] * own_value
    heads_out = mixed.astype(BF16).reshape(row_count, query_cols)
    layer_out = experts(
        nz,
        ny,
        heads_out,
        tokens,
        norm_gain_mix[None, :],
        norm_gain_ffn[None, :],
        routes,
        route_weights,
        w_out,
        expert_gate,
        expert_up,
        expert_down,
    )
    return (layer_out, new_keys, new_values, new_log_gate)


def solution(mesh):
    placed = (
        P("ep", None),
        P(),
        P("ep", "tp"),
        P("ep", "tp"),
        P("ep", "tp"),
        P(None, "tp"),
        P("tp"),
        P("ep", "tp", None),
        P("ep", "tp", None),
        P("ep", "tp", None),
        P("ep"),
        P("tp", None),
        P(),
        P(),
        P(None, ("ep", "tp")),
        P(None, ("ep", "tp")),
        P(("ep", "tp"), None),
        P("ep", None),
        P("ep", None),
    )
    nz = mesh.shape["ep"] // (NX * NC)
    return jax.shard_map(
        functools.partial(body, nz, mesh.shape["tp"]),
        mesh=mesh,
        in_specs=placed,
        out_specs=(P("ep", "tp"), P("ep", "tp"), P("ep", "tp"), P("ep", "tp")),
        check_vma=False,
    )
```

time: 247 us -> 101 us (0.41)
  waiting for transfers between devices: 126 us -> 0 us
  Pallas kernels: 0 us -> 81.1 us
  blocking collectives: 58 us -> 0 us
  starting transfers between devices: 14.9 us -> 0 us
  between operations: 14.3 us -> 0.71 us
  matrix products: 16.6 us -> 6.47 us
    pallas_call x0 -> x2, Pallas kernels: none -> 81.1 us  [the longest x1 56.8 us: experts(): pl.pallas_call(functools.partial(experts_kernel, nz, ny), out_shape=jax.S...]
    all_gather x1 -> x0, waiting for transfers between devices: 72.8 us -> none  [sent_together(): out = lax.all_gather(both, axis, axis=dim, tiled=True)]
    all_to_all x1 -> x0, blocking collectives: 58 us -> none  [body(): lax.all_to_all(outgoing, 'ep', split_axis=0, concat_axis=0, tiled=True)]
    reduce_scatter x1 -> x0, waiting for transfers between devices: 27.7 us -> none  [body(): lax.psum_scatter(expert_part.astype(jnp.bfloat16), 'tp', scatter_dimensio...]
    all_to_all x2 -> x0, waiting for transfers between devices: 25.7 us -> none  [the longest x1 16.7 us: body(): lax.all_to_all(col_share.reshape(sources, slots, -1).astype(jnp.bfloat16)...]
    all_to_all x2 -> x0, starting transfers between devices: 14.9 us -> none  [the longest x1 10.4 us: body(): lax.all_to_all(col_share.reshape(sources, slots, -1).astype(jnp.bfloat16)...]
    dot_general x7 -> x1, matrix products: 12.2 us -> 1.76 us  [body(): jnp.dot(normed, w_forget, preferred_element_type=F32) + forget_bias]
  transfers between devices with their start and end apart: 4 -> 0, of which waited for: 4 -> 0; matrix products, arithmetic and copies ran while one was open for 4% -> 0% of each run, Pallas kernels for 0% -> 0%
where the time goes in v1:
time: 101 us; the launch traced here: 99.7 us
  Pallas kernels  81.1 us (80%)
  other arithmetic  7.57 us (7%)
  matrix products  6.47 us (6%)
  local copies, waits for them, and re-layouts  3.85 us (4%)
    pallas_call x1, Pallas kernels, experts(): pl.pallas_call(functools.partial(experts_kernel, nz, ny), out_shape=jax.S...  56.8 us
    pallas_call x1, Pallas kernels, project(): pl.pallas_call(functools.partial(project_kernel, nz), out_shape=jax.Shape...  24.3 us
    dot_general x1, matrix products, body(): jnp.einsum('bkgd,bkdl->bkgl', query_heads, key_heads, preferred_element_t...  3.46 us
    unnamed x11, local copies, waits for them, and re-layouts  2.77 us

profile of v1, /device:TPU:32, one launch (start us, length us, event | category | flops | bytes accessed | tf_op | source)
XLA Modules:
  0.0 99.7 jit_solution(7713196571139908712)
XLA Ops:
  0.6 0.0 copy-start
  0.6 1.5 %pad_maximum_fusion.w_own = bf16[32,640]{1,0:T(8,128)(2,1)} fusion(bf16[32,64]{1,0:T(8,128)(2,1)} %param.23, bf16[32,64]{1,0:T(8,128)(2,1)} %param.22, bf16[32,512]{1,0:T(8,128)(2,1)} %param.21), kind=kLoop, calls=%fused_computation.24 | loop fusion | flops 122880 | bytes 81920 | tf_op jit(solution)/shard_map/concatenate | solution.py:421
  2.1 24.3 %project.1 = f32[32,640]{1,0:T(8,128)} custom-call(bf16[32,2048]{1,0:T(8,128)(2,1)} %tokens.3, f32[1,2048]{1,0:T(1,128)} %bitcast.10, bf16[32,640]{1,0:T(8,128)(2,1)} %pad_maximum_fusion.w_own), custom_call_target="tpu_custom_call" | custom-call | tf_op jit(solution)/shard_map/project/pallas_call | solution.py:111
  26.4 0.9 convert.6
  27.3 0.7 fusion.19
  28.0 0.1 reshape.143
  28.1 0.1 multiply_reduce_fusion.1
  28.2 0.1 reshape.141
  28.3 0.7 broadcast_add_fusion
  29.0 0.1 fusion.13
  29.1 1.4 %multiply_reduce_fusion = f32[32,8]{1,0:T(8,128)S(1)} fusion(f32[32,8,1024]{2,1,0:T(8,128)} %param.28, f32[32,1024]{1,0:T(8,128)S(1)} %fusion.13), kind=kLoop, calls=%fused_computation.9 | loop fusion | flops 524032 | bytes 1180672 | tf_op jit(solution)/shard_map/reduce_sum | solution.py:445
  30.5 0.1 copy.26
  30.5 1.0 %fusion.7 = f32[32]{0:T(128)S(1)} fusion(bf16[32,2048]{1,0:T(8,128)(2,1)} %tokens.3), kind=kLoop, calls=%fused_computation.15 | loop fusion | flops 196576 | bytes 131200 | tf_op jit(solution)/shard_map/reduce_sum | solution.py:25
  31.6 0.0 copy-done
  31.6 1.8 %fusion.21 = (f32[32,8]{0,1:T(8,128)S(1)}, f32[32,8]{0,1:T(8,128)}) fusion(f32[32,8]{0,1:T(8,128)S(1)} %copy.26, f32[8]{0:T(128)} %param.25, bf16[2048,8]{0,1:T(8,128)(2,1)S(1)} %copy-done, bf16[32,2048]{1,0:T(8,128)(2,1)} %tokens.3, f32[2048]{0:T(1024)} %param.20, f32[32]{0:T(128)S(1)} %add_rsqrt_fusion), kind=kOutput, calls=%fused_computation.37 | convolution fusion | flops 1313280 | bytes 175264 | tf_op jit(solution)/shard_map/dot_general | solution.py:427
  33.3 0.1 copy.27
  33.4 0.0 copy-start.3
  33.4 0.9 iota_compare_fusion.1
  34.3 3.5 %fusion.22 = (f32[32,8]{1,0:T(8,128)S(1)}, f32[32,8,1024]{2,1,0:T(8,128)S(1)}) fusion(f32[32,8,1024]{2,1,0:T(8,128)} %param.28, f32[32,8]{1,0:T(8,128)S(1)} %copy.27, bf16[32,8,64]{2,1,0:T(8,128)(2,1)S(1)} %reshape.141, bf16[32,64,1024]{2,1,0:T(8,128)(2,1)} %param.26, pred[32,1024]{1,0:T(8,128)(4,1)S(1)} %iota_compare_fusion.1), kind=kOutput, calls=%fused_computation.38 | convolution fusion | flops 34864896 | bytes 6359040 | tf_op jit(solution)/shard_map/bkgd,bkdl->bkgl/dot_general | solution.py:437
  37.8 0.0 copy-start.1
  37.8 0.0 copy-start.2
  37.8 0.3 fusion.4
  38.1 0.0 copy-done.3
  38.1 1.2 %fusion.2 = bf16[32,8,64]{2,1,0:T(8,128)(2,1)S(1)} fusion(bf16[32,64,1024]{2,1,0:T(8,128)(2,1)S(1)} %copy-done.3, f32[32,8,1024]{2,1,0:T(8,128)S(1)} %get-tuple-element.17, f32[32,8]{1,0:T(8,128)S(1)} %get-tuple-element.9, f32[32,8]{1,0:T(8,128)S(1)} %multiply_maximum_fusion, f32[32,64]{1,0:T(8,128)S(1)} %get-tuple-element.4, f32[32,8]{1,0:T(8,128)S(1)} %get-tuple-element.8), kind=kOutput, calls=%fused_computation.4 | convolution fusion | flops 34390016 | bytes 5286912 | tf_op jit(solution)/shard_map/bkgl,bkdl->bkgd/dot_general | solution.py:457
  39.4 0.7 reshape.142.heads
  40.1 0.0 copy-done.1
  40.1 0.7 copy.28.routes
  40.8 0.0 copy-done.2
  40.8 0.7 copy.29.route_weights
  41.5 56.8 %experts.1 = bf16[32,512]{1,0:T(8,128)(2,1)} custom-call(bf16[32,512]{1,0:T(8,128)(2,1)} %reshape.142.heads, bf16[32,2048]{1,0:T(8,128)(2,1)} %tokens.3, f32[1,2048]{1,0:T(1,128)} %bitcast.8, f32[1,2048]{1,0:T(1,128)} %bitcast.9, s32[32,2]{1,0:T(8,128)} %copy.28.routes, s32[2,32]{1,0:T(2,128)} %bitcast.11, f32[32,2]{1,0:T(8,128)} %copy.29.route_weights, ...), custom_call_target="tpu_custom_call" | custom-call | tf_op jit(solution)/shard_map/experts/pallas_call | solution.py:353
  98.3 1.4 %copy.31 = bf16[32,512]{1,0:T(8,128)(2,1)} copy(bf16[32,512]{1,0:T(8,128)(2,1)} %experts.1) | data formatting | bytes 65536
  (4 shorter events, 0.0 us)
Async XLA Ops:
  0.6 30.9 %copy-start = (bf16[2048,8]{0,1:T(8,128)(2,1)S(1)}, bf16[2048,8]{0,1:T(8,128)(2,1)}, u32[]{:S(2)}) copy-start(bf16[2048,8]{0,1:T(8,128)(2,1)} %param.24) | copy-start | bytes 98308
  33.4 4.7 %copy-start.3 = (bf16[32,64,1024]{2,1,0:T(8,128)(2,1)S(1)}, bf16[32,64,1024]{2,1,0:T(8,128)(2,1)}, u32[]{:S(2)}) copy-start(bf16[32,64,1024]{2,1,0:T(8,128)(2,1)} %param.27) | copy-start | bytes 12582916
  37.8 2.3 %copy-start.1 = (s32[32,2]{0,1:T(2,128)S(1)}, s32[32,2]{0,1:T(2,128)}, u32[]{:S(2)}) copy-start(s32[32,2]{0,1:T(2,128)} %param.36) | copy-start | bytes 772
  37.8 3.0 %copy-start.2 = (f32[32,2]{0,1:T(2,128)S(1)}, f32[32,2]{0,1:T(2,128)}, u32[]{:S(2)}) copy-start(f32[32,2]{0,1:T(2,128)} %param.37) | copy-start | bytes 772

commit v2 on v0

v2 whole, which is shorter than its diff:
```python
import functools

import jax
import jax.numpy as jnp
from jax import lax
from jax.experimental import pallas as pl
from jax.experimental.pallas import tpu as pltpu
from jax.sharding import PartitionSpec as P

HEAD_DIM = 64
NX = 4
NC = 2
FLAT = NX * NC
SLOTS = 8
TOGETHER = 8
EPSILON = 1e-06
MASKED = -1e30
MESH = pl.DeviceIdType.MESH
F32 = jnp.float32
BF16 = jnp.bfloat16
EXACT = lax.Precision.HIGHEST
ACROSS = (((1,), (1,)), ((), ()))


def rms_scaled(field, gain_vector):
    return (
        field * lax.rsqrt(jnp.mean(field * field, axis=-1, keepdims=True) + EPSILON) * gain_vector
    )


def log_sigmoid(v):
    return jnp.minimum(v, 0.0) - jnp.log1p(jnp.exp(-jnp.abs(v)))


def dot(a, b):
    return jnp.dot(a, b, preferred_element_type=F32)


def dot_across(a, b, precision=None):
    return lax.dot_general(a, b, ACROSS, precision=precision, preferred_element_type=F32)


def iota(shape, dim):
    return lax.broadcasted_iota(jnp.int32, shape, dim)


def ones_where(mask):
    return jnp.where(mask, 1.0, 0.0).astype(F32)


def remote(src, dst, send, recv, ep, y):
    return pltpu.make_async_remote_copy(
        src_ref=src, dst_ref=dst, send_sem=send, recv_sem=recv, device_id=(ep, y), device_id_type=MESH
    )


def slotted(first, second, expert_of, slot_of, axis):
    in_first, in_second = first == expert_of, second == expert_of
    member = ones_where(in_first | in_second)
    rows = member.shape[axis]
    if axis == 0:
        before = ones_where(iota((rows, rows), 1) < iota((rows, rows), 0)).astype(BF16)
        earlier = dot(before, member.astype(BF16))
    else:
        before = ones_where(iota((rows, rows), 0) < iota((rows, rows), 1)).astype(BF16)
        earlier = dot(member.astype(BF16), before)
    return jnp.where(earlier == slot_of.astype(F32), member, 0.0), in_first, in_second


def nearest_first(n):
    return [(p + 1) // 2 if p % 2 else (n - p // 2) % n for p in range(n)]


def layer_kernel(nz, ny, *refs):
    (tokens, gain_attn, w_query, w_key, w_value, w_forget, forget_bias, lengths) = refs[:8]
    (gain_mix, gain_ffn, routes_across, weights_across) = refs[8:12]
    (keys, values, logcum, w_out, gate, up, down) = refs[12:19]
    (out, new_keys, new_values, new_log_gate) = refs[19:23]
    (keys_v, values_v, logcum_v, wo_v, gate_v, up_v, down_v) = refs[23:30]
    (w_own, w_in, normed, t_in, sums, p_out, p_in) = refs[30:37]
    (query_s, own_value_s, columns_s, heads_s) = refs[37:41]
    (mix_out, mix_in, mixed_res, packed, z_in, x_in, share_out, share_in, back_out, back_in) = refs[41:51]
    (load_sem, w_sem, t_sem, p_sem, pair_sem, y_sem, z_sem, x_sem, s_sem, b_sem) = refs[51:]

    ep, y = lax.axis_index("ep"), lax.axis_index("tp")
    z = lax.div(ep, FLAT)
    at = lax.rem(ep, FLAT)
    x, c = lax.div(at, NC), lax.rem(at, NC)
    rows, width = tokens.shape
    part = width // ny
    query_cols = w_query.shape[1]
    heads = query_cols // HEAD_DIM
    stacked = rows * heads
    span = keys.shape[2]

    def chip(dz, dx):
        return lax.rem(z + dz, nz) * FLAT + lax.rem(x + dx, NX) * NC + c

    def row_peer(d):
        return z * FLAT + lax.rem(at + d, FLAT)

    def y_peer(d):
        return lax.rem(y + d, ny)

    partner = ep + 1 - 2 * c
    barrier = pltpu.get_barrier_semaphore()

    def signal(ep_to, y_to):
        pl.semaphore_signal(barrier, inc=1, device_id=(ep_to, y_to), device_id_type=MESH)

    for dz in range(nz):
        for dx in range(NX):
            if dz or dx:
                signal(chip(dz, dx), y)
    for dx in range(NX):
        signal(z * FLAT + lax.rem(x + dx, NX) * NC + 1 - c, y)
    for d in range(1, ny):
        signal(ep, y_peer(d))

    loads = [
        pltpu.make_async_copy(src, dst, load_sem.at[i])
        for i, (src, dst) in enumerate(
            (
                (keys, keys_v),
                (logcum, logcum_v),
                (values, values_v),
                (w_out, wo_v),
                (gate, gate_v.at[0]),
                (up, up_v.at[0]),
                (down, down_v.at[0]),
            )
        )
    ]
    for load in loads:
        load.start()

    w_own[:, :query_cols] = w_query[...]
    w_own[:, query_cols : query_cols + HEAD_DIM] = w_key[...]
    w_own[:, query_cols + HEAD_DIM :] = w_value[...]
    scaled = rms_scaled(tokens[...].astype(F32), gain_attn[...]).astype(BF16)
    slab = width // nz
    for k in range(nz):
        normed[k] = scaled[:, k * slab : (k + 1) * slab]
    pl.semaphore_wait(barrier, nz * NX - 1 + NX + ny - 1)

    near_first = nearest_first(nz)
    far_first = near_first[:0:-1]
    w_copies = [
        remote(w_own, w_in.at[at], w_sem.at[0, d], w_sem.at[1, d], row_peer(d), y)
        for d in range(1, FLAT)
    ]
    t_copies = [
        remote(normed.at[lax.rem(z + d, nz)], t_in.at[d], t_sem.at[0, d], t_sem.at[1, d], chip(d, 0), y)
        for d in far_first
    ]
    for copy in t_copies + w_copies:
        copy.start()
    w_in[at] = w_own[...]
    t_in[0] = normed[z]
    log_gate = log_sigmoid(dot_across(scaled, w_forget[...]) + forget_bias[...])
    new_log_gate[...] = log_sigmoid(
        dot_across(w_forget[...], scaled) + jnp.transpose(jnp.broadcast_to(forget_bias[...], (rows, heads)))
    )
    for copy in w_copies + t_copies:
        copy.wait_recv()
    product = dot(
        t_in[...].reshape(nz * rows, slab), w_in[...].reshape(FLAT * w_own.shape[0], w_own.shape[1])
    )
    for d in range(1, nz):
        p_out[d] = product[d * rows : (d + 1) * rows].astype(BF16)
    sums[...] = product[:rows]
    p_copies = [
        remote(p_out.at[d], p_in.at[d], p_sem.at[0, d], p_sem.at[1, d], chip(nz - d, 0), y)
        for d in far_first
    ]
    for copy in p_copies:
        copy.start()
    shape = (nz * 2 * SLOTS, rows)
    lane = iota(shape, 0)
    expert_of = 2 * lax.rem(z + lane // (2 * SLOTS), nz) + (lane // SLOTS) % 2
    picking, _, _ = slotted(routes_across[0:1, :], routes_across[1:2, :], expert_of, lane % SLOTS, 1)
    picking = picking.astype(BF16)
    unit = ones_where(iota((rows, rows), 0) == iota((rows, rows), 1))
    routes = dot_across(unit, routes_across[...].astype(F32)).astype(jnp.int32)
    weights = dot_across(unit, weights_across[...], EXACT)
    shape = (rows, nz * NX * SLOTS)
    lane = iota(shape, 1)
    place = lane // (NX * SLOTS)
    dz_of = jnp.where(place % 2 == 1, (place + 1) // 2, nz - place // 2)
    expert_of = 2 * lax.rem(z + dz_of, nz) + lax.rem(x + (lane // SLOTS) % NX, NX) // 2
    weighing, in_first, in_second = slotted(routes[:, 0:1], routes[:, 1:2], expert_of, lane % SLOTS, 0)
    weighing = weighing * (
        jnp.where(in_first, weights[:, 0:1], 0.0) + jnp.where(in_second, weights[:, 1:2], 0.0)
    )
    coarse = weighing.astype(BF16)
    fine = (weighing - coarse.astype(F32)).astype(BF16)
    repeat = ones_where(iota((stacked, rows), 0) // heads == iota((stacked, rows), 1))
    gate_of = jnp.dot(repeat, log_gate, precision=EXACT, preferred_element_type=F32)
    own_head = iota((stacked, heads), 1) == iota((stacked, heads), 0) % heads
    gate_of = jnp.sum(jnp.where(own_head, gate_of, 0.0), axis=1, keepdims=True)
    repeat = repeat.astype(BF16)
    fold = ones_where(iota((query_cols, HEAD_DIM), 0) % HEAD_DIM == iota((query_cols, HEAD_DIM), 1))
    fold = fold.astype(BF16)
    own_part = iota((stacked, query_cols), 1) // HEAD_DIM == iota((stacked, query_cols), 0) % heads
    total = sums[...]
    for copy in p_copies[::-1]:
        copy.wait_recv()
    for d in range(1, nz):
        total = total + p_in[d].astype(F32)
    projected = total.astype(BF16)
    new_key = projected[:, query_cols : query_cols + HEAD_DIM]
    new_value = projected[:, query_cols + HEAD_DIM :]
    new_keys[...] = new_key
    new_values[...] = new_value

    pair_copies = [
        remote(src, dst.at[1], pair_sem.at[0, i], pair_sem.at[1, i], partner, y)
        for i, (src, dst) in enumerate(((gate, gate_v), (up, up_v), (down, down_v)))
    ]
    for copy in pair_copies:
        copy.start()
    spread = jnp.where(own_part, dot(repeat, projected[:, :query_cols]), 0.0).astype(BF16)
    query_of = dot(spread, fold) * HEAD_DIM ** (-0.5)
    query_s[...] = query_of
    columns_s[:, 0:1] = jnp.sum(query_of * dot(repeat, new_key), axis=1, keepdims=True)
    columns_s[:, 1:2] = gate_of
    own_value_s[...] = dot(repeat, new_value)
    for load in loads[:3]:
        load.wait()

    def attend(step, carry):
        group = []
        for j in range(TOGETHER):
            b = step * TOGETHER + j
            at_rows = pl.ds(pl.multiple_of(b * heads, heads), heads)
            score = dot(query_s[at_rows, :].astype(BF16), keys_v[b])
            group.append((b, at_rows, score))
        for j, (b, at_rows, score) in enumerate(group):
            cum = logcum_v[b]
            length = lengths[b]
            position = iota((heads, span), 1)
            last = jnp.sum(jnp.where(position == length - 1, cum, 0.0), axis=1, keepdims=True)
            own = columns_s[at_rows, 0:1]
            shift = (last + columns_s[at_rows, 1:2]) - cum
            past = jnp.where(position < length, score + shift, MASKED)
            peak = jnp.maximum(jnp.max(past, axis=1, keepdims=True), own)
            past = jnp.exp(past - peak)
            own = jnp.exp(own - peak)
            group[j] = (b, at_rows, past, own, jnp.sum(past, axis=1, keepdims=True) + own)
        for b, at_rows, past, own, norm in group:
            mixed = dot_across(past.astype(BF16), values_v[b]) + own * own_value_s[at_rows, :]
            heads_s[at_rows, :] = mixed / norm
        return carry

    lax.fori_loop(0, rows // TOGETHER, attend, 0)
    spread = jnp.where(own_part, dot_across(heads_s[...].astype(BF16), fold), 0.0).astype(BF16)
    gather = ones_where(iota((rows, stacked), 1) // heads == iota((rows, stacked), 0)).astype(BF16)
    heads_out = dot(gather, spread).astype(BF16)
    loads[3].wait()
    mix_out[...] = dot(heads_out, wo_v[...]).astype(BF16)

    y_copies = [
        remote(mix_out, mix_in.at[d], y_sem.at[0, d], y_sem.at[1, d], ep, y_peer(d)) for d in range(1, ny)
    ]
    for copy in y_copies:
        copy.start()
    for copy in w_copies + t_copies + p_copies:
        copy.wait_send()
    for load in loads[4:]:
        load.wait()
    mix = mix_out[...].astype(F32)
    for i, copy in enumerate(y_copies):
        copy.wait_recv()
        mix = mix + mix_in[i + 1].astype(F32)
    mixed = tokens[...].astype(F32) + rms_scaled(mix, gain_mix[...])
    for k in range(ny):
        mixed_res[k] = mixed[:, k * part : (k + 1) * part]
    ffn_in = rms_scaled(mixed, gain_ffn[...]).astype(BF16)
    packed[...] = dot(picking, ffn_in).astype(BF16).reshape(nz, 2, SLOTS, width)

    z_copies = [None] + [
        remote(packed.at[d], z_in.at[p], z_sem.at[0, p], z_sem.at[1, p], chip(d, 0), y)
        for p, d in enumerate(near_first)
        if p
    ]
    for copy in z_copies[1:]:
        copy.start()
    z_in[0] = packed[0]
    x_copies, s_copies, b_copies = {}, {}, []
    chunks = [(0, 3), (3, 5), (5, 7), (7, 8)] if nz == 8 else [(p, p + 1) for p in range(nz)]

    def forward(chunk):
        for p in range(*chunk):
            if p:
                z_copies[p].wait_recv()
            for dx in range(1, NX):
                half = lax.rem(x + dx, NX) // 2
                x_copies[p, dx] = remote(
                    z_in.at[p, half], x_in.at[p, dx], x_sem.at[0, p, dx], x_sem.at[1, p, dx], chip(0, dx), y
                )
                x_copies[p, dx].start()
            x_in[p, 0] = z_in[p, x // 2]

    def multiply(chunk):
        lo, hi = chunk
        for p in range(lo, hi):
            for dx in range(1, NX):
                x_copies[p, dx].wait_recv()
        if lo == 0:
            for copy in pair_copies:
                copy.wait_recv()
        count = (hi - lo) * NX * SLOTS
        first = lo * NX * SLOTS
        arrived = x_in[lo:hi].reshape(count, width)
        hidden = []
        for k in range(NC):
            gate_part = dot(arrived, gate_v[k])
            up_part = dot(arrived, up_v[k])
            hidden.append((gate_part / (1.0 + jnp.exp(-gate_part)) * up_part).astype(BF16))
        for j in range(ny):
            cols = slice(j * part, (j + 1) * part)
            share = dot(hidden[0], down_v[0, :, cols]) + dot(hidden[1], down_v[1, :, cols])
            share_out[j, first : first + count] = share.astype(BF16)
        for d in range(1, ny):
            s_copies[lo, d] = remote(
                share_out.at[y_peer(d), pl.ds(first, count)],
                share_in.at[d, pl.ds(first, count)],
                s_sem.at[0, lo, d],
                s_sem.at[1, lo, d],
                ep,
                y_peer(d),
            )
            s_copies[lo, d].start()

    def give_back(chunk):
        lo, hi = chunk
        count = (hi - lo) * NX * SLOTS
        here = pl.ds(lo * NX * SLOTS, count)
        total = share_out[y, here].astype(F32)
        for d in range(1, ny):
            s_copies[lo, d].wait_recv()
            total = total + share_in[d, here].astype(F32)
        back_out[lo:hi] = total.astype(BF16).reshape(hi - lo, NX, SLOTS, part)
        for p in range(lo, hi):
            for dx in range(NX):
                if p or dx:
                    copy = remote(
                        back_out.at[p, dx],
                        back_in.at[p, dx],
                        b_sem.at[0, p, dx],
                        b_sem.at[1, p, dx],
                        chip(nz - near_first[p], NX - dx),
                        y,
                    )
                    copy.start()
                    b_copies.append(copy)
                else:
                    back_in[0, 0] = back_out[0, 0]

    forward(chunks[0])
    for i, chunk in enumerate(chunks):
        if i + 1 < len(chunks):
            forward(chunks[i + 1])
        multiply(chunk)
        if i:
            give_back(chunks[i - 1])
    give_back(chunks[-1])
    for copy in y_copies + pair_copies + z_copies[1:] + list(x_copies.values()) + list(s_copies.values()):
        copy.wait_send()
    for copy in b_copies:
        copy.wait_recv()
    returned = back_in[...].reshape(nz * NX * SLOTS, part)
    out[...] = (mixed_res[y] + (dot(coarse, returned) + dot(fine, returned))).astype(BF16)
    for copy in b_copies:
        copy.wait_send()


def body(
    nz,
    ny,
    tokens,
    norm_gain_attn,
    w_query,
    w_key,
    w_value,
    w_forget,
    forget_bias,
    cache_keys,
    cache_values,
    cache_logcum,
    lengths,
    w_out,
    norm_gain_mix,
    norm_gain_ffn,
    expert_gate,
    expert_up,
    expert_down,
    routes,
    route_weights,
):
    rows, width = tokens.shape
    part = width // ny
    query_cols = w_query.shape[1]
    cols = query_cols + w_key.shape[1] + w_value.shape[1]
    heads = query_cols // HEAD_DIM
    hidden = expert_gate.shape[1]
    depth = w_query.shape[0]
    stacked = rows * heads
    lanes = nz * NX * SLOTS
    vmem = pl.BlockSpec(memory_space=pltpu.VMEM)
    kept = pl.BlockSpec(memory_space=pl.ANY)
    smem = pl.BlockSpec(memory_space=pltpu.SMEM)

    def dma(*shape):
        return pltpu.SemaphoreType.DMA((2, *shape))

    layer_out, new_keys, new_values, new_log_gate = pl.pallas_call(
        functools.partial(layer_kernel, nz, ny),
        out_shape=(
            jax.ShapeDtypeStruct((rows, part), BF16),
            jax.ShapeDtypeStruct((rows, HEAD_DIM), BF16),
            jax.ShapeDtypeStruct((rows, HEAD_DIM), BF16),
            jax.ShapeDtypeStruct((heads, rows), F32),
        ),
        in_specs=[vmem] * 7 + [smem] + [vmem] * 4 + [kept] * 7,
        out_specs=(vmem,) * 4,
        scratch_shapes=[
            pltpu.VMEM(cache_keys.shape, BF16),
            pltpu.VMEM(cache_values.shape, BF16),
            pltpu.VMEM(cache_logcum.shape, F32),
            pltpu.VMEM(w_out.shape, BF16),
            pltpu.VMEM((NC, width, hidden), BF16),
            pltpu.VMEM((NC, width, hidden), BF16),
            pltpu.VMEM((NC, hidden, width), BF16),
            pltpu.VMEM((depth, cols), BF16),
            pltpu.VMEM((FLAT, depth, cols), BF16),
            pltpu.VMEM((nz, rows, width // nz), BF16),
            pltpu.VMEM((nz, rows, width // nz), BF16),
            pltpu.VMEM((rows, cols), F32),
            pltpu.VMEM((nz, rows, cols), BF16),
            pltpu.VMEM((nz, rows, cols), BF16),
            pltpu.VMEM((stacked, HEAD_DIM), F32),
            pltpu.VMEM((stacked, HEAD_DIM), F32),
            pltpu.VMEM((stacked, 2), F32),
            pltpu.VMEM((stacked, HEAD_DIM), F32),
            pltpu.VMEM((rows, width), BF16),
            pltpu.VMEM((ny, rows, width), BF16),
            pltpu.VMEM((ny, rows, part), F32),
            pltpu.VMEM((nz, 2, SLOTS, width), BF16),
            pltpu.VMEM((nz, 2, SLOTS, width), BF16),
            pltpu.VMEM((nz, NX, SLOTS, width), BF16),
            pltpu.VMEM((ny, lanes, part), BF16),
            pltpu.VMEM((ny, lanes, part), BF16),
            pltpu.VMEM((nz, NX, SLOTS, part), BF16),
            pltpu.VMEM((nz, NX, SLOTS, part), BF16),
            pltpu.SemaphoreType.DMA((7,)),
            dma(FLAT),
            dma(nz),
            dma(nz),
            dma(3),
            dma(ny),
            dma(nz),
            dma(nz, NX),
            dma(nz, ny),
            dma(nz, NX),
        ],
        compiler_params=pltpu.CompilerParams(collective_id=0, has_side_effects=True),
        name="layer",
    )(
        tokens,
        norm_gain_attn[None, :],
        w_query,
        w_key,
        w_value,
        w_forget.T,
        forget_bias[None, :],
        lengths,
        norm_gain_mix[None, :],
        norm_gain_ffn[None, :],
        routes.T,
        route_weights.T,
        cache_keys,
        cache_values,
        cache_logcum,
        w_out,
        expert_gate,
        expert_up,
        expert_down,
    )
    return layer_out, new_keys, new_values, new_log_gate.T


def solution(mesh):
    placed = (
        P("ep", None),
        P(),
        P("ep", "tp"),
        P("ep", "tp"),
        P("ep", "tp"),
        P(None, "tp"),
        P("tp"),
        P("ep", "tp", None),
        P("ep", "tp", None),
        P("ep", "tp", None),
        P("ep"),
        P("tp", None),
        P(),
        P(),
        P(None, ("ep", "tp")),
        P(None, ("ep", "tp")),
        P(("ep", "tp"), None),
        P("ep", None),
        P("ep", None),
    )
    nz = mesh.shape["ep"] // FLAT
    return jax.shard_map(
        functools.partial(body, nz, mesh.shape["tp"]),
        mesh=mesh,
        in_specs=placed,
        out_specs=(P("ep", "tp"), P("ep", "tp"), P("ep", "tp"), P("ep", "tp")),
        check_vma=False,
    )
```

time: 247 us -> 84.3 us (0.34); the launches traced: 244 us -> 84 us
  waiting for transfers between devices: 126 us -> 0 us
  Pallas kernels: 0 us -> 78.1 us
  blocking collectives: 58 us -> 0 us
  matrix products: 16.6 us -> 0 us
  starting transfers between devices: 14.9 us -> 0 us
  between operations: 14.3 us -> 0.65 us
  other arithmetic: 9.9 us -> 0 us
    pallas_call x0 -> x1, Pallas kernels: none -> 78.1 us  [body(): pl.pallas_call(functools.partial(layer_kernel, nz, ny), out_shape=(jax.Sh...]
    all_gather x1 -> x0, waiting for transfers between devices: 72.8 us -> none  [sent_together(): out = lax.all_gather(both, axis, axis=dim, tiled=True)]
    all_to_all x1 -> x0, blocking collectives: 58 us -> none  [body(): lax.all_to_all(outgoing, 'ep', split_axis=0, concat_axis=0, tiled=True)]
    reduce_scatter x1 -> x0, waiting for transfers between devices: 27.7 us -> none  [body(): lax.psum_scatter(expert_part.astype(jnp.bfloat16), 'tp', scatter_dimensio...]
    all_to_all x2 -> x0, waiting for transfers between devices: 25.7 us -> none  [the longest x1 16.7 us: body(): lax.all_to_all(col_share.reshape(sources, slots, -1).astype(jnp.bfloat16)...]
    dot_general x9 -> x0, matrix products: 16.6 us -> none  [the longest x1 5.83 us: body(): jnp.dot(hidden, expert_down, preferred_element_type=jnp.float32)]
    all_to_all x2 -> x0, starting transfers between devices: 14.9 us -> none  [the longest x1 10.4 us: body(): lax.all_to_all(col_share.reshape(sources, slots, -1).astype(jnp.bfloat16)...]
    reduce_sum x10 -> x0, other arithmetic: 5.05 us -> none  [the longest x3 1.47 us: rms_scaled(): jnp.mean(field * field, axis=-1, keepdims=True) + EPSILON]
  transfers between devices with their start and end apart: 4 -> 0, of which waited for: 4 -> 0; matrix products, arithmetic and copies ran while one was open for 4% -> 0% of each run, Pallas kernels for 0% -> 0%
where the time goes in v2:
time: 84.3 us; the launch traced here: 84 us
  Pallas kernels  78.1 us (93%)
  local copies, waits for them, and re-layouts  5.24 us (6%)
    pallas_call x1, Pallas kernels, body(): pl.pallas_call(functools.partial(layer_kernel, nz, ny), out_shape=(jax.Sh...  78.1 us
    unnamed x4, local copies, waits for them, and re-layouts  5.24 us

profile of v2, /device:TPU:32, one launch (start us, length us, event | category | flops | bytes accessed | tf_op | source)
XLA Modules:
  0.0 84.0 jit_solution(16307235278748724296)
XLA Ops:
  0.6 78.1 %layer.1 = (bf16[32,512]{1,0:T(8,128)(2,1)}, bf16[32,64]{1,0:T(8,128)(2,1)}, bf16[32,64]{1,0:T(8,128)(2,1)}, f32[8,32]{1,0:T(8,128)}) custom-call(bf16[32,2048]{1,0:T(8,128)(2,1)} %refs_0_.1, f32[1,2048]{1,0:T(1,128)} %bitcast.9, bf16[32,512]{1,0:T(8,128)(2,1)} %refs_2_.1, bf16[32,64]{1,0:T(8,128)(2,1)} %refs_3_.1, bf16[32,64]{1,0:T(8,128)(2,1)} %refs_4_.1, ...), custom_call_target="tpu_custom_call" | custom-call | tf_op jit(solution)/shard_map/layer/pallas_call | solution.py:417
  78.7 1.4 %copy.27 = bf16[32,512]{1,0:T(8,128)(2,1)} copy(bf16[32,512]{1,0:T(8,128)(2,1)} %get-tuple-element.16) | data formatting | bytes 65536
  80.1 1.3 %copy.28 = bf16[32,64]{1,0:T(8,128)(2,1)} copy(bf16[32,64]{1,0:T(8,128)(2,1)} %get-tuple-element.17) | data formatting | bytes 8192
  81.4 1.3 %copy.29 = bf16[32,64]{1,0:T(8,128)(2,1)} copy(bf16[32,64]{1,0:T(8,128)(2,1)} %get-tuple-element.18) | data formatting | bytes 8192
  82.7 1.3 %copy.30 = f32[32,8]{0,1:T(8,128)} copy(f32[32,8]{0,1:T(8,128)} %bitcast.12) | data formatting | bytes 2048

commit v3 on v2

--- a/solution.py
+++ b/solution.py
@@ -13,6 +13,7 @@
 FLAT = NX * NC
 SLOTS = 8
 TOGETHER = 8
+HALVES = 2
 EPSILON = 1e-06
 MASKED = -1e30
 MESH = pl.DeviceIdType.MESH
@@ -108,12 +109,10 @@
     def signal(ep_to, y_to):
         pl.semaphore_signal(barrier, inc=1, device_id=(ep_to, y_to), device_id_type=MESH)
 
-    for dz in range(nz):
-        for dx in range(NX):
-            if dz or dx:
-                signal(chip(dz, dx), y)
-    for dx in range(NX):
-        signal(z * FLAT + lax.rem(x + dx, NX) * NC + 1 - c, y)
+    for d in range(1, nz):
+        signal(chip(d, 0), y)
+    for d in range(1, FLAT):
+        signal(row_peer(d), y)
     for d in range(1, ny):
         signal(ep, y_peer(d))
 
@@ -141,7 +140,7 @@
     slab = width // nz
     for k in range(nz):
         normed[k] = scaled[:, k * slab : (k + 1) * slab]
-    pl.semaphore_wait(barrier, nz * NX - 1 + NX + ny - 1)
+    pl.semaphore_wait(barrier, nz - 1 + FLAT - 1 + ny - 1)
 
     near_first = nearest_first(nz)
     far_first = near_first[:0:-1]
@@ -252,26 +251,39 @@
             heads_s[at_rows, :] = mixed / norm
         return carry
 
-    lax.fori_loop(0, rows // TOGETHER, attend, 0)
-    spread = jnp.where(own_part, dot_across(heads_s[...].astype(BF16), fold), 0.0).astype(BF16)
-    gather = ones_where(iota((rows, stacked), 1) // heads == iota((rows, stacked), 0)).astype(BF16)
-    heads_out = dot(gather, spread).astype(BF16)
-    loads[3].wait()
-    mix_out[...] = dot(heads_out, wo_v[...]).astype(BF16)
-
-    y_copies = [
-        remote(mix_out, mix_in.at[d], y_sem.at[0, d], y_sem.at[1, d], ep, y_peer(d)) for d in range(1, ny)
-    ]
-    for copy in y_copies:
-        copy.start()
+    y_copies = []
+    count = rows // HALVES
+    gather = ones_where(iota((count, count * heads), 1) // heads == iota((count, count * heads), 0)).astype(BF16)
+    for half in range(HALVES):
+        steps = count // TOGETHER
+        lax.fori_loop(half * steps, (half + 1) * steps, attend, 0)
+        lo = half * count * heads
+        mixed = heads_s[lo : lo + count * heads, :].astype(BF16)
+        spread = jnp.where(own_part[: count * heads], dot_across(mixed, fold), 0.0).astype(BF16)
+        heads_out = dot(gather, spread).astype(BF16)
+        if half == 0:
+            loads[3].wait()
+        mix_out[half] = dot(heads_out, wo_v[...]).astype(BF16)
+        for d in range(1, ny):
+            copy = remote(
+                mix_out.at[half],
+                mix_in.at[d, half],
+                y_sem.at[0, d, half],
+                y_sem.at[1, d, half],
+                ep,
+                y_peer(d),
+            )
+            copy.start()
+            y_copies.append(copy)
     for copy in w_copies + t_copies + p_copies:
         copy.wait_send()
     for load in loads[4:]:
         load.wait()
-    mix = mix_out[...].astype(F32)
-    for i, copy in enumerate(y_copies):
+    mix = mix_out[...].reshape(rows, width).astype(F32)
+    for copy in y_copies:
         copy.wait_recv()
-        mix = mix + mix_in[i + 1].astype(F32)
+    for d in range(1, ny):
+        mix = mix + mix_in[d].reshape(rows, width).astype(F32)
     mixed = tokens[...].astype(F32) + rms_scaled(mix, gain_mix[...])
     for k in range(ny):
         mixed_res[k] = mixed[:, k * part : (k + 1) * part]
@@ -373,6 +385,11 @@
     out[...] = (mixed_res[y] + (dot(coarse, returned) + dot(fine, returned))).astype(BF16)
     for copy in b_copies:
         copy.wait_send()
+
+
+def write_kernel(*refs):
+    for src, dst in zip(refs[:4], refs[4:]):
+        dst[...] = src[...]
 
 
 def body(
@@ -414,7 +431,7 @@
     def dma(*shape):
         return pltpu.SemaphoreType.DMA((2, *shape))
 
-    layer_out, new_keys, new_values, new_log_gate = pl.pallas_call(
+    results = pl.pallas_call(
         functools.partial(layer_kernel, nz, ny),
         out_shape=(
             jax.ShapeDtypeStruct((rows, part), BF16),
@@ -443,8 +460,8 @@
             pltpu.VMEM((stacked, HEAD_DIM), F32),
             pltpu.VMEM((stacked, 2), F32),
             pltpu.VMEM((stacked, HEAD_DIM), F32),
-            pltpu.VMEM((rows, width), BF16),
-            pltpu.VMEM((ny, rows, width), BF16),
+            pltpu.VMEM((HALVES, rows // HALVES, width), BF16),
+            pltpu.VMEM((ny, HALVES, rows // HALVES, width), BF16),
             pltpu.VMEM((ny, rows, part), F32),
             pltpu.VMEM((nz, 2, SLOTS, width), BF16),
             pltpu.VMEM((nz, 2, SLOTS, width), BF16),
@@ -458,7 +475,7 @@
             dma(nz),
             dma(nz),
             dma(3),
-            dma(ny),
+            dma(ny, HALVES),
             dma(nz),
             dma(nz, NX),
             dma(nz, ny),
@@ -487,6 +504,13 @@
         expert_up,
         expert_down,
     )
+    layer_out, new_keys, new_values, new_log_gate = pl.pallas_call(
+        write_kernel,
+        out_shape=tuple(jax.ShapeDtypeStruct(a.shape, a.dtype) for a in results),
+        in_specs=(vmem,) * 4,
+        out_specs=(vmem,) * 4,
+        name="write",
+    )(*results)
     return layer_out, new_keys, new_values, new_log_gate.T
 
 

time: 84.3 us -> 77.9 us (0.924)
  local copies, waits for them, and re-layouts: 5.24 us -> 0 us
  Pallas kernels: 78.1 us -> 76.9 us
    unnamed x4 -> x0, local copies, waits for them, and re-layouts: 5.24 us -> none
    pallas_call x1, Pallas kernels: 78.1 us -> 75.5 us  [body(): pl.pallas_call(functools.partial(layer_kernel, nz, ny), out_shape=(jax.Sh...]
    pallas_call x0 -> x1, Pallas kernels: none -> 1.41 us  [body(): pl.pallas_call(write_kernel, out_shape=tuple((jax.ShapeDtypeStruct(a.shap...]
where the time goes in v3:
time: 77.9 us; the launch traced here: 77.5 us
  Pallas kernels  76.9 us (99%)
    pallas_call x1, Pallas kernels, body(): pl.pallas_call(functools.partial(layer_kernel, nz, ny), out_shape=(jax.Sh...  75.5 us

profile of v3, /device:TPU:32, one launch (start us, length us, event | category | flops | bytes accessed | tf_op | source)
XLA Modules:
  0.0 77.5 jit_solution(5928691658743259194)
XLA Ops:
  0.6 75.5 %layer.1 = (bf16[32,512]{1,0:T(8,128)(2,1)}, bf16[32,64]{1,0:T(8,128)(2,1)}, bf16[32,64]{1,0:T(8,128)(2,1)}, f32[8,32]{1,0:T(8,128)}) custom-call(bf16[32,2048]{1,0:T(8,128)(2,1)} %refs_0_.1, f32[1,2048]{1,0:T(1,128)} %bitcast.9, bf16[32,512]{1,0:T(8,128)(2,1)} %refs_2_.1, bf16[32,64]{1,0:T(8,128)(2,1)} %refs_3_.1, bf16[32,64]{1,0:T(8,128)(2,1)} %refs_4_.1, ...), custom_call_target="tpu_custom_call" | custom-call | tf_op jit(solution)/shard_map/layer/pallas_call | solution.py:434
  76.1 1.4 %write.1 = (bf16[32,512]{1,0:T(8,128)(2,1)}, bf16[32,64]{1,0:T(8,128)(2,1)}, bf16[32,64]{1,0:T(8,128)(2,1)}, f32[8,32]{1,0:T(8,128)}) custom-call(bf16[32,512]{1,0:T(8,128)(2,1)} %get-tuple-element.12.refs_0_, bf16[32,64]{1,0:T(8,128)(2,1)} %get-tuple-element.13.refs_1_, bf16[32,64]{1,0:T(8,128)(2,1)} %get-tuple-element.14.refs_2_, ...), custom_call_target="tpu_custom_call" | custom-call | tf_op jit(solution)/shard_map/write/pallas_call | solution.py:507

commit v4 on v3

--- a/solution.py
+++ b/solution.py
@@ -13,7 +13,12 @@
 FLAT = NX * NC
 SLOTS = 8
 TOGETHER = 8
-HALVES = 2
+CHUNKS = ((0, 1), (1, 3), (3, 5), (5, 7), (7, 8))
+SCHEDULE = (
+    *(("x", 0), ("y", 1), ("y", 2), ("m", 0), ("x", 1), ("x", 2), ("y", 3), ("y", 4), ("x", 3), ("x", 4), ("y", 5)),
+    *(("y", 6), ("m", 1), ("x", 5), ("x", 6), ("y", 7), ("r", 0), ("m", 2), ("x", 7), ("r", 1), ("m", 3), ("r", 2)),
+    *(("m", 4), ("r", 3), ("r", 4)),
+)
 EPSILON = 1e-06
 MASKED = -1e30
 MESH = pl.DeviceIdType.MESH
@@ -68,20 +73,26 @@
     return jnp.where(earlier == slot_of.astype(F32), member, 0.0), in_first, in_second
 
 
-def nearest_first(n):
+def near_order(n):
     return [(p + 1) // 2 if p % 2 else (n - p // 2) % n for p in range(n)]
 
 
+def of_both(sides, weights, k):
+    depth, cols = 2 * weights.shape[3], weights.shape[4]
+    return sum(dot(side, weights[k, :, i].reshape(depth, cols)) for i, side in enumerate(sides))
+
+
 def layer_kernel(nz, ny, *refs):
-    (tokens, gain_attn, w_query, w_key, w_value, w_forget, forget_bias, lengths) = refs[:8]
-    (gain_mix, gain_ffn, routes_across, weights_across) = refs[8:12]
-    (keys, values, logcum, w_out, gate, up, down) = refs[12:19]
-    (out, new_keys, new_values, new_log_gate) = refs[19:23]
-    (keys_v, values_v, logcum_v, wo_v, gate_v, up_v, down_v) = refs[23:30]
-    (w_own, w_in, normed, t_in, sums, p_out, p_in) = refs[30:37]
-    (query_s, own_value_s, columns_s, heads_s) = refs[37:41]
-    (mix_out, mix_in, mixed_res, packed, z_in, x_in, share_out, share_in, back_out, back_in) = refs[41:51]
-    (load_sem, w_sem, t_sem, p_sem, pair_sem, y_sem, z_sem, x_sem, s_sem, b_sem) = refs[51:]
+    small_hbm, (keys, values, logcum, w_out, gate, up, down), lengths = refs[:11], refs[11:18], refs[18]
+    results_hbm, small, results_v = refs[19:23], refs[23:34], refs[34:38]
+    (tokens, gain_attn, w_query, w_key, w_value, w_forget, forget_bias) = small[:7]
+    (gain_mix, gain_ffn, routes_across, weights_across) = small[7:]
+    (out, new_keys, new_values, new_log_gate) = results_v
+    (keys_v, values_v, logcum_v, wo_v, gate_v, up_v, down_v) = refs[38:45]
+    (w_own, w_in, normed, t_in, sums, p_out, p_in) = refs[45:52]
+    (query_s, own_value_s, columns_s, heads_s, own_kv) = refs[52:57]
+    (mix_out, mix_in, mixed_res, packed, z_in, x_in, share_out, share_in, back_out, back_in) = refs[57:67]
+    (small_sem, result_sem, load_sem, w_sem, t_sem, p_sem, pair_sem, y_sem, z_sem, x_sem, g_sem, s_sem, b_sem) = refs[67:]
 
     ep, y = lax.axis_index("ep"), lax.axis_index("tp")
     z = lax.div(ep, FLAT)
@@ -105,6 +116,7 @@
 
     partner = ep + 1 - 2 * c
     barrier = pltpu.get_barrier_semaphore()
+    parity = lax.rem(y, 2)
 
     def signal(ep_to, y_to):
         pl.semaphore_signal(barrier, inc=1, device_id=(ep_to, y_to), device_id_type=MESH)
@@ -116,6 +128,15 @@
     for d in range(1, ny):
         signal(ep, y_peer(d))
 
+    fetches = [
+        pltpu.make_async_copy(src, dst, small_sem.at[i]) for i, (src, dst) in enumerate(zip(small_hbm, small))
+    ]
+    for fetch in fetches:
+        fetch.start()
+    writes = [
+        pltpu.make_async_copy(src, dst, result_sem.at[i])
+        for i, (src, dst) in enumerate(zip(results_v, results_hbm))
+    ]
     loads = [
         pltpu.make_async_copy(src, dst, load_sem.at[i])
         for i, (src, dst) in enumerate(
@@ -130,8 +151,8 @@
             )
         )
     ]
-    for load in loads:
-        load.start()
+    for fetch in fetches:
+        fetch.wait()
 
     w_own[:, :query_cols] = w_query[...]
     w_own[:, query_cols : query_cols + HEAD_DIM] = w_key[...]
@@ -142,8 +163,8 @@
         normed[k] = scaled[:, k * slab : (k + 1) * slab]
     pl.semaphore_wait(barrier, nz - 1 + FLAT - 1 + ny - 1)
 
-    near_first = nearest_first(nz)
-    far_first = near_first[:0:-1]
+    offsets = near_order(nz)
+    far_first = offsets[:0:-1]
     w_copies = [
         remote(w_own, w_in.at[at], w_sem.at[0, d], w_sem.at[1, d], row_peer(d), y)
         for d in range(1, FLAT)
@@ -154,26 +175,38 @@
     ]
     for copy in t_copies + w_copies:
         copy.start()
+    for load in loads:
+        load.start()
     w_in[at] = w_own[...]
     t_in[0] = normed[z]
     log_gate = log_sigmoid(dot_across(scaled, w_forget[...]) + forget_bias[...])
     new_log_gate[...] = log_sigmoid(
         dot_across(w_forget[...], scaled) + jnp.transpose(jnp.broadcast_to(forget_bias[...], (rows, heads)))
     )
+    writes[3].start()
     for copy in w_copies + t_copies:
         copy.wait_recv()
     product = dot(
         t_in[...].reshape(nz * rows, slab), w_in[...].reshape(FLAT * w_own.shape[0], w_own.shape[1])
     )
-    for d in range(1, nz):
-        p_out[d] = product[d * rows : (d + 1) * rows].astype(BF16)
+    steps = rows // TOGETHER
+    for step in range(steps):
+        for d in range(1, nz):
+            first = d * rows + step * TOGETHER
+            p_out[step, d] = product[first : first + TOGETHER].astype(BF16)
     sums[...] = product[:rows]
-    p_copies = [
-        remote(p_out.at[d], p_in.at[d], p_sem.at[0, d], p_sem.at[1, d], chip(nz - d, 0), y)
-        for d in far_first
-    ]
-    for copy in p_copies:
-        copy.start()
+    p_copies = {}
+    for step in range(steps):
+        for d in far_first:
+            p_copies[step, d] = remote(
+                p_out.at[step, d],
+                p_in.at[step, d],
+                p_sem.at[0, step, d],
+                p_sem.at[1, step, d],
+                chip(nz - d, 0),
+                y,
+            )
+            p_copies[step, d].start()
     shape = (nz * 2 * SLOTS, rows)
     lane = iota(shape, 0)
     expert_of = 2 * lax.rem(z + lane // (2 * SLOTS), nz) + (lane // SLOTS) % 2
@@ -197,37 +230,37 @@
     gate_of = jnp.dot(repeat, log_gate, precision=EXACT, preferred_element_type=F32)
     own_head = iota((stacked, heads), 1) == iota((stacked, heads), 0) % heads
     gate_of = jnp.sum(jnp.where(own_head, gate_of, 0.0), axis=1, keepdims=True)
-    repeat = repeat.astype(BF16)
     fold = ones_where(iota((query_cols, HEAD_DIM), 0) % HEAD_DIM == iota((query_cols, HEAD_DIM), 1))
     fold = fold.astype(BF16)
-    own_part = iota((stacked, query_cols), 1) // HEAD_DIM == iota((stacked, query_cols), 0) % heads
-    total = sums[...]
-    for copy in p_copies[::-1]:
-        copy.wait_recv()
-    for d in range(1, nz):
-        total = total + p_in[d].astype(F32)
-    projected = total.astype(BF16)
-    new_key = projected[:, query_cols : query_cols + HEAD_DIM]
-    new_value = projected[:, query_cols + HEAD_DIM :]
-    new_keys[...] = new_key
-    new_values[...] = new_value
-
+    columns_s[:, 1:2] = gate_of
+    some = TOGETHER * heads
+    repeat = ones_where(iota((some, TOGETHER), 0) // heads == iota((some, TOGETHER), 1)).astype(BF16)
+    gather = ones_where(iota((TOGETHER, some), 1) // heads == iota((TOGETHER, some), 0)).astype(BF16)
+    own_part = iota((some, query_cols), 1) // HEAD_DIM == iota((some, query_cols), 0) % heads
     pair_copies = [
         remote(src, dst.at[1], pair_sem.at[0, i], pair_sem.at[1, i], partner, y)
         for i, (src, dst) in enumerate(((gate, gate_v), (up, up_v), (down, down_v)))
     ]
-    for copy in pair_copies:
-        copy.start()
-    spread = jnp.where(own_part, dot(repeat, projected[:, :query_cols]), 0.0).astype(BF16)
-    query_of = dot(spread, fold) * HEAD_DIM ** (-0.5)
-    query_s[...] = query_of
-    columns_s[:, 0:1] = jnp.sum(query_of * dot(repeat, new_key), axis=1, keepdims=True)
-    columns_s[:, 1:2] = gate_of
-    own_value_s[...] = dot(repeat, new_value)
-    for load in loads[:3]:
-        load.wait()
-
-    def attend(step, carry):
+
+    def prepare(step):
+        at_rows = slice(step * TOGETHER, (step + 1) * TOGETHER)
+        at_heads = slice(step * some, (step + 1) * some)
+        for d in far_first:
+            p_copies[step, d].wait_recv()
+        total = sums[at_rows, :]
+        for d in range(1, nz):
+            total = total + p_in[step, d].astype(F32)
+        projected = total.astype(BF16)
+        own_kv[at_rows, :] = projected[:, query_cols:].astype(F32)
+        new_key = projected[:, query_cols : query_cols + HEAD_DIM]
+        new_value = projected[:, query_cols + HEAD_DIM :]
+        spread = jnp.where(own_part, dot(repeat, projected[:, :query_cols]), 0.0).astype(BF16)
+        query_of = dot(spread, fold) * HEAD_DIM ** (-0.5)
+        query_s[at_heads, :] = query_of
+        columns_s[at_heads, 0:1] = jnp.sum(query_of * dot(repeat, new_key), axis=1, keepdims=True)
+        own_value_s[at_heads, :] = dot(repeat, new_value)
+
+    def attend(step):
         group = []
         for j in range(TOGETHER):
             b = step * TOGETHER + j
@@ -249,33 +282,39 @@
         for b, at_rows, past, own, norm in group:
             mixed = dot_across(past.astype(BF16), values_v[b]) + own * own_value_s[at_rows, :]
             heads_s[at_rows, :] = mixed / norm
-        return carry
 
     y_copies = []
-    count = rows // HALVES
-    gather = ones_where(iota((count, count * heads), 1) // heads == iota((count, count * heads), 0)).astype(BF16)
-    for half in range(HALVES):
-        steps = count // TOGETHER
-        lax.fori_loop(half * steps, (half + 1) * steps, attend, 0)
-        lo = half * count * heads
-        mixed = heads_s[lo : lo + count * heads, :].astype(BF16)
-        spread = jnp.where(own_part[: count * heads], dot_across(mixed, fold), 0.0).astype(BF16)
+    for step in range(steps):
+        prepare(step)
+        if step == 0:
+            for load in loads[:3]:
+                load.wait()
+        if step == steps - 1:
+            for copy in pair_copies:
+                copy.start()
+        attend(step)
+        mixed = heads_s[step * some : (step + 1) * some, :].astype(BF16)
+        spread = jnp.where(own_part, dot_across(mixed, fold), 0.0).astype(BF16)
         heads_out = dot(gather, spread).astype(BF16)
-        if half == 0:
+        if step == 0:
             loads[3].wait()
-        mix_out[half] = dot(heads_out, wo_v[...]).astype(BF16)
+        mix_out[step] = dot(heads_out, wo_v[...]).astype(BF16)
         for d in range(1, ny):
             copy = remote(
-                mix_out.at[half],
-                mix_in.at[d, half],
-                y_sem.at[0, d, half],
-                y_sem.at[1, d, half],
+                mix_out.at[step],
+                mix_in.at[d, step],
+                y_sem.at[0, d, step],
+                y_sem.at[1, d, step],
                 ep,
                 y_peer(d),
             )
             copy.start()
             y_copies.append(copy)
-    for copy in w_copies + t_copies + p_copies:
+    new_keys[...] = own_kv[:, :HEAD_DIM].astype(BF16)
+    new_values[...] = own_kv[:, HEAD_DIM:].astype(BF16)
+    writes[1].start()
+    writes[2].start()
+    for copy in w_copies + t_copies + list(p_copies.values()):
         copy.wait_send()
     for load in loads[4:]:
         load.wait()
@@ -288,30 +327,43 @@
     for k in range(ny):
         mixed_res[k] = mixed[:, k * part : (k + 1) * part]
     ffn_in = rms_scaled(mixed, gain_ffn[...]).astype(BF16)
-    packed[...] = dot(picking, ffn_in).astype(BF16).reshape(nz, 2, SLOTS, width)
+    quarters = [ffn_in[:, k * part : (k + 1) * part] for k in range(ny)]
+    sides = [jnp.concatenate((quarters[k], quarters[k + 2]), axis=1) for k in range(2)]
+    side = jnp.where(parity == 0, sides[0], sides[1])
+    packed[...] = dot(picking, side).astype(BF16).reshape(nz, 2, SLOTS, width // 2)
 
     z_copies = [None] + [
-        remote(packed.at[d], z_in.at[p], z_sem.at[0, p], z_sem.at[1, p], chip(d, 0), y)
-        for p, d in enumerate(near_first)
+        remote(packed.at[d], z_in.at[parity, p], z_sem.at[0, p], z_sem.at[1, p], chip(d, 0), y)
+        for p, d in enumerate(offsets)
         if p
     ]
     for copy in z_copies[1:]:
         copy.start()
-    z_in[0] = packed[0]
-    x_copies, s_copies, b_copies = {}, {}, []
-    chunks = [(0, 3), (3, 5), (5, 7), (7, 8)] if nz == 8 else [(p, p + 1) for p in range(nz)]
-
-    def forward(chunk):
-        for p in range(*chunk):
-            if p:
-                z_copies[p].wait_recv()
-            for dx in range(1, NX):
-                half = lax.rem(x + dx, NX) // 2
-                x_copies[p, dx] = remote(
-                    z_in.at[p, half], x_in.at[p, dx], x_sem.at[0, p, dx], x_sem.at[1, p, dx], chip(0, dx), y
-                )
-                x_copies[p, dx].start()
-            x_in[p, 0] = z_in[p, x // 2]
+    for k in range(2):
+        own = dot(picking[: 2 * SLOTS], sides[k]).astype(BF16)
+        z_in[k, 0] = own.reshape(2, SLOTS, width // 2)
+    x_copies, g_copies, s_copies, b_copies = {}, {}, {}, []
+    chunks = CHUNKS
+
+    def hand_over(p):
+        z_copies[p].wait_recv()
+        for i, d in enumerate((ny - 1, 1)):
+            block = z_in.at[parity, p, i]
+            g_copies[p, i] = remote(block, block, g_sem.at[0, p, i], g_sem.at[1, p, i], ep, y_peer(d))
+            g_copies[p, i].start()
+
+    def forward(p):
+        if p:
+            for i in range(2):
+                g_copies[p, i].wait_recv()
+        for dx in range(1, NX):
+            half = lax.rem(x + dx, NX) // 2
+            x_copies[p, dx] = remote(
+                z_in.at[:, p, half], x_in.at[:, p, dx], x_sem.at[0, p, dx], x_sem.at[1, p, dx], chip(0, dx), y
+            )
+            x_copies[p, dx].start()
+        for k in range(2):
+            x_in[k, p, 0] = z_in[k, p, x // 2]
 
     def multiply(chunk):
         lo, hi = chunk
@@ -323,11 +375,11 @@
                 copy.wait_recv()
         count = (hi - lo) * NX * SLOTS
         first = lo * NX * SLOTS
-        arrived = x_in[lo:hi].reshape(count, width)
+        arrived = [x_in[k, lo:hi].reshape(count, width // 2) for k in range(2)]
         hidden = []
         for k in range(NC):
-            gate_part = dot(arrived, gate_v[k])
-            up_part = dot(arrived, up_v[k])
+            gate_part = of_both(arrived, gate_v, k)
+            up_part = of_both(arrived, up_v, k)
             hidden.append((gate_part / (1.0 + jnp.exp(-gate_part)) * up_part).astype(BF16))
         for j in range(ny):
             cols = slice(j * part, (j + 1) * part)
@@ -361,7 +413,7 @@
                         back_in.at[p, dx],
                         b_sem.at[0, p, dx],
                         b_sem.at[1, p, dx],
-                        chip(nz - near_first[p], NX - dx),
+                        chip(nz - offsets[p], NX - dx),
                         y,
                     )
                     copy.start()
@@ -369,22 +421,28 @@
                 else:
                     back_in[0, 0] = back_out[0, 0]
 
-    forward(chunks[0])
-    for i, chunk in enumerate(chunks):
-        if i + 1 < len(chunks):
-            forward(chunks[i + 1])
-        multiply(chunk)
-        if i:
-            give_back(chunks[i - 1])
-    give_back(chunks[-1])
-    for copy in y_copies + pair_copies + z_copies[1:] + list(x_copies.values()) + list(s_copies.values()):
+    for step, argument in SCHEDULE:
+        if step == "x":
+            forward(argument)
+        elif step == "y":
+            hand_over(argument)
+        elif step == "m":
+            multiply(chunks[argument])
+        else:
+            give_back(chunks[argument])
+    for copy in y_copies + pair_copies + z_copies[1:] + list(x_copies.values()):
+        copy.wait_send()
+    for copy in list(g_copies.values()) + list(s_copies.values()):
         copy.wait_send()
     for copy in b_copies:
         copy.wait_recv()
     returned = back_in[...].reshape(nz * NX * SLOTS, part)
     out[...] = (mixed_res[y] + (dot(coarse, returned) + dot(fine, returned))).astype(BF16)
+    writes[0].start()
     for copy in b_copies:
         copy.wait_send()
+    for write in writes:
+        write.wait()
 
 
 def write_kernel(*refs):
@@ -424,6 +482,7 @@
     depth = w_query.shape[0]
     stacked = rows * heads
     lanes = nz * NX * SLOTS
+    steps = rows // TOGETHER
     vmem = pl.BlockSpec(memory_space=pltpu.VMEM)
     kept = pl.BlockSpec(memory_space=pl.ANY)
     smem = pl.BlockSpec(memory_space=pltpu.SMEM)
@@ -431,59 +490,7 @@
     def dma(*shape):
         return pltpu.SemaphoreType.DMA((2, *shape))
 
-    results = pl.pallas_call(
-        functools.partial(layer_kernel, nz, ny),
-        out_shape=(
-            jax.ShapeDtypeStruct((rows, part), BF16),
-            jax.ShapeDtypeStruct((rows, HEAD_DIM), BF16),
-            jax.ShapeDtypeStruct((rows, HEAD_DIM), BF16),
-            jax.ShapeDtypeStruct((heads, rows), F32),
-        ),
-        in_specs=[vmem] * 7 + [smem] + [vmem] * 4 + [kept] * 7,
-        out_specs=(vmem,) * 4,
-        scratch_shapes=[
-            pltpu.VMEM(cache_keys.shape, BF16),
-            pltpu.VMEM(cache_values.shape, BF16),
-            pltpu.VMEM(cache_logcum.shape, F32),
-            pltpu.VMEM(w_out.shape, BF16),
-            pltpu.VMEM((NC, width, hidden), BF16),
-            pltpu.VMEM((NC, width, hidden), BF16),
-            pltpu.VMEM((NC, hidden, width), BF16),
-            pltpu.VMEM((depth, cols), BF16),
-            pltpu.VMEM((FLAT, depth, cols), BF16),
-            pltpu.VMEM((nz, rows, width // nz), BF16),
-            pltpu.VMEM((nz, rows, width // nz), BF16),
-            pltpu.VMEM((rows, cols), F32),
-            pltpu.VMEM((nz, rows, cols), BF16),
-            pltpu.VMEM((nz, rows, cols), BF16),
-            pltpu.VMEM((stacked, HEAD_DIM), F32),
-            pltpu.VMEM((stacked, HEAD_DIM), F32),
-            pltpu.VMEM((stacked, 2), F32),
-            pltpu.VMEM((stacked, HEAD_DIM), F32),
-            pltpu.VMEM((HALVES, rows // HALVES, width), BF16),
-            pltpu.VMEM((ny, HALVES, rows // HALVES, width), BF16),
-            pltpu.VMEM((ny, rows, part), F32),
-            pltpu.VMEM((nz, 2, SLOTS, width), BF16),
-            pltpu.VMEM((nz, 2, SLOTS, width), BF16),
-            pltpu.VMEM((nz, NX, SLOTS, width), BF16),
-            pltpu.VMEM((ny, lanes, part), BF16),
-            pltpu.VMEM((ny, lanes, part), BF16),
-            pltpu.VMEM((nz, NX, SLOTS, part), BF16),
-            pltpu.VMEM((nz, NX, SLOTS, part), BF16),
-            pltpu.SemaphoreType.DMA((7,)),
-            dma(FLAT),
-            dma(nz),
-            dma(nz),
-            dma(3),
-            dma(ny, HALVES),
-            dma(nz),
-            dma(nz, NX),
-            dma(nz, ny),
-            dma(nz, NX),
-        ],
-        compiler_params=pltpu.CompilerParams(collective_id=0, has_side_effects=True),
-        name="layer",
-    )(
+    small = (
         tokens,
         norm_gain_attn[None, :],
         w_query,
@@ -491,18 +498,79 @@
         w_value,
         w_forget.T,
         forget_bias[None, :],
-        lengths,
         norm_gain_mix[None, :],
         norm_gain_ffn[None, :],
         routes.T,
         route_weights.T,
+    )
+    shapes = (
+        jax.ShapeDtypeStruct((rows, part), BF16),
+        jax.ShapeDtypeStruct((rows, HEAD_DIM), BF16),
+        jax.ShapeDtypeStruct((rows, HEAD_DIM), BF16),
+        jax.ShapeDtypeStruct((heads, rows), F32),
+    )
+    results = pl.pallas_call(
+        functools.partial(layer_kernel, nz, ny),
+        out_shape=shapes,
+        in_specs=[kept] * 18 + [smem],
+        out_specs=(kept,) * 4,
+        scratch_shapes=[
+            *(pltpu.VMEM(a.shape, a.dtype) for a in (*small, *shapes)),
+            pltpu.VMEM(cache_keys.shape, BF16),
+            pltpu.VMEM(cache_values.shape, BF16),
+            pltpu.VMEM(cache_logcum.shape, F32),
+            pltpu.VMEM(w_out.shape, BF16),
+            pltpu.VMEM((NC, 2, 2, part, hidden), BF16),
+            pltpu.VMEM((NC, 2, 2, part, hidden), BF16),
+            pltpu.VMEM((NC, hidden, width), BF16),
+            pltpu.VMEM((depth, cols), BF16),
+            pltpu.VMEM((FLAT, depth, cols), BF16),
+            pltpu.VMEM((nz, rows, width // nz), BF16),
+            pltpu.VMEM((nz, rows, width // nz), BF16),
+            pltpu.VMEM((rows, cols), F32),
+            pltpu.VMEM((steps, nz, TOGETHER, cols), BF16),
+            pltpu.VMEM((steps, nz, TOGETHER, cols), BF16),
+            pltpu.VMEM((stacked, HEAD_DIM), F32),
+            pltpu.VMEM((stacked, HEAD_DIM), F32),
+            pltpu.VMEM((stacked, 2), F32),
+            pltpu.VMEM((stacked, HEAD_DIM), F32),
+            pltpu.VMEM((rows, 2 * HEAD_DIM), F32),
+            pltpu.VMEM((steps, TOGETHER, width), BF16),
+            pltpu.VMEM((ny, steps, TOGETHER, width), BF16),
+            pltpu.VMEM((ny, rows, part), F32),
+            pltpu.VMEM((nz, 2, SLOTS, width // 2), BF16),
+            pltpu.VMEM((2, nz, 2, SLOTS, width // 2), BF16),
+            pltpu.VMEM((2, nz, NX, SLOTS, width // 2), BF16),
+            pltpu.VMEM((ny, lanes, part), BF16),
+            pltpu.VMEM((ny, lanes, part), BF16),
+            pltpu.VMEM((nz, NX, SLOTS, part), BF16),
+            pltpu.VMEM((nz, NX, SLOTS, part), BF16),
+            pltpu.SemaphoreType.DMA((len(small),)),
+            pltpu.SemaphoreType.DMA((len(shapes),)),
+            pltpu.SemaphoreType.DMA((7,)),
+            dma(FLAT),
+            dma(nz),
+            dma(steps, nz),
+            dma(3),
+            dma(ny, steps),
+            dma(nz),
+            dma(nz, NX),
+            dma(nz, 2),
+            dma(nz, ny),
+            dma(nz, NX),
+        ],
+        compiler_params=pltpu.CompilerParams(collective_id=0, has_side_effects=True),
+        name="layer",
+    )(
+        *small,
         cache_keys,
         cache_values,
         cache_logcum,
         w_out,
-        expert_gate,
-        expert_up,
+        expert_gate.reshape(2, 2, part, hidden),
+        expert_up.reshape(2, 2, part, hidden),
         expert_down,
+        lengths,
     )
     layer_out, new_keys, new_values, new_log_gate = pl.pallas_call(
         write_kernel,

time: 77.9 us -> 73.6 us (0.945)
  Pallas kernels: 76.9 us -> 72.4 us
    pallas_call x1, Pallas kernels: 75.5 us -> 71 us  [body(): pl.pallas_call(functools.partial(layer_kernel, nz, ny), out_shape=shapes,...]
where the time goes in v4:
time: 73.6 us; the launch traced here: 73.1 us
  Pallas kernels  72.4 us (98%)
    pallas_call x1, Pallas kernels, body(): pl.pallas_call(functools.partial(layer_kernel, nz, ny), out_shape=shapes,...  71 us

profile of v4, /device:TPU:32, one launch (start us, length us, event | category | flops | bytes accessed | tf_op | source)
XLA Modules:
  0.0 73.1 jit_solution(3905048119452637031)
XLA Ops:
  0.6 71.0 %layer.1 = (bf16[32,512]{1,0:T(8,128)(2,1)}, bf16[32,64]{1,0:T(8,128)(2,1)}, bf16[32,64]{1,0:T(8,128)(2,1)}, f32[8,32]{1,0:T(8,128)}) custom-call(bf16[32,2048]{1,0:T(8,128)(2,1)} %refs_0_.1, f32[1,2048]{1,0:T(1,128)} %bitcast.13, bf16[32,512]{1,0:T(8,128)(2,1)} %refs_2_.1, bf16[32,64]{1,0:T(8,128)(2,1)} %refs_3_.1, bf16[32,64]{1,0:T(8,128)(2,1)} %refs_4_.1, ...), custom_call_target="tpu_custom_call" | custom-call | tf_op jit(solution)/shard_map/layer/pallas_call | solution.py:512
  71.7 1.4 %write.1 = (bf16[32,512]{1,0:T(8,128)(2,1)}, bf16[32,64]{1,0:T(8,128)(2,1)}, bf16[32,64]{1,0:T(8,128)(2,1)}, f32[8,32]{1,0:T(8,128)}) custom-call(bf16[32,512]{1,0:T(8,128)(2,1)} %get-tuple-element.12.refs_0_, bf16[32,64]{1,0:T(8,128)(2,1)} %get-tuple-element.13.refs_1_, bf16[32,64]{1,0:T(8,128)(2,1)} %get-tuple-element.14.refs_2_, ...), custom_call_target="tpu_custom_call" | custom-call | tf_op jit(solution)/shard_map/write/pallas_call | solution.py:575

commit v5 on v4

--- a/solution.py
+++ b/solution.py
@@ -13,11 +13,11 @@
 FLAT = NX * NC
 SLOTS = 8
 TOGETHER = 8
+HANDED = 8
 CHUNKS = ((0, 1), (1, 3), (3, 5), (5, 7), (7, 8))
 SCHEDULE = (
-    *(("x", 0), ("y", 1), ("y", 2), ("m", 0), ("x", 1), ("x", 2), ("y", 3), ("y", 4), ("x", 3), ("x", 4), ("y", 5)),
-    *(("y", 6), ("m", 1), ("x", 5), ("x", 6), ("y", 7), ("r", 0), ("m", 2), ("x", 7), ("r", 1), ("m", 3), ("r", 2)),
-    *(("m", 4), ("r", 3), ("r", 4)),
+    *(("x", 0), ("x", 1), ("x", 2), ("m", 0), ("x", 3), ("x", 4), ("x", 5), ("x", 6), ("x", 7),),
+    *(("m", 1), ("m", 2), ("m", 3), ("m", 4), ("r", 0), ("r", 1), ("r", 2), ("r", 3), ("r", 4),),
 )
 EPSILON = 1e-06
 MASKED = -1e30
@@ -329,19 +329,21 @@
     ffn_in = rms_scaled(mixed, gain_ffn[...]).astype(BF16)
     quarters = [ffn_in[:, k * part : (k + 1) * part] for k in range(ny)]
     sides = [jnp.concatenate((quarters[k], quarters[k + 2]), axis=1) for k in range(2)]
-    side = jnp.where(parity == 0, sides[0], sides[1])
-    packed[...] = dot(picking, side).astype(BF16).reshape(nz, 2, SLOTS, width // 2)
-
-    z_copies = [None] + [
-        remote(packed.at[d], z_in.at[parity, p], z_sem.at[0, p], z_sem.at[1, p], chip(d, 0), y)
-        for p, d in enumerate(offsets)
-        if p
-    ]
+    for k in range(2):
+        packed[k] = dot(picking, sides[k]).astype(BF16).reshape(nz, 2, SLOTS, width // 2)
+
+    z_copies = [None]
+    for p, d in enumerate(offsets):
+        if p:
+            kind = slice(None) if p < HANDED else parity
+            copy = remote(
+                packed.at[kind, d], z_in.at[kind, p], z_sem.at[0, p], z_sem.at[1, p], chip(d, 0), y
+            )
+            z_copies.append(copy)
     for copy in z_copies[1:]:
         copy.start()
     for k in range(2):
-        own = dot(picking[: 2 * SLOTS], sides[k]).astype(BF16)
-        z_in[k, 0] = own.reshape(2, SLOTS, width // 2)
+        z_in[k, 0] = packed[k, 0]
     x_copies, g_copies, s_copies, b_copies = {}, {}, {}, []
     chunks = CHUNKS
 
@@ -353,9 +355,11 @@
             g_copies[p, i].start()
 
     def forward(p):
-        if p:
+        if p >= HANDED:
             for i in range(2):
                 g_copies[p, i].wait_recv()
+        elif p:
+            z_copies[p].wait_recv()
         for dx in range(1, NX):
             half = lax.rem(x + dx, NX) // 2
             x_copies[p, dx] = remote(
@@ -538,7 +542,7 @@
             pltpu.VMEM((steps, TOGETHER, width), BF16),
             pltpu.VMEM((ny, steps, TOGETHER, width), BF16),
             pltpu.VMEM((ny, rows, part), F32),
-            pltpu.VMEM((nz, 2, SLOTS, width // 2), BF16),
+            pltpu.VMEM((2, nz, 2, SLOTS, width // 2), BF16),
             pltpu.VMEM((2, nz, 2, SLOTS, width // 2), BF16),
             pltpu.VMEM((2, nz, NX, SLOTS, width // 2), BF16),
             pltpu.VMEM((ny, lanes, part), BF16),

time: 73.6 us -> 69 us (0.938)
  Pallas kernels: 72.4 us -> 68 us
    pallas_call x1, Pallas kernels: 71 us -> 66.5 us  [body(): pl.pallas_call(functools.partial(layer_kernel, nz, ny), out_shape=shapes,...]
where the time goes in v5:
time: 69 us; the launch traced here: 68.6 us
  Pallas kernels  68 us (99%)
    pallas_call x1, Pallas kernels, body(): pl.pallas_call(functools.partial(layer_kernel, nz, ny), out_shape=shapes,...  66.5 us
    pallas_call x1, Pallas kernels, body(): pl.pallas_call(write_kernel, out_shape=tuple((jax.ShapeDtypeStruct(a.shap...  1.41 us

profile of v5, /device:TPU:32, one launch (start us, length us, event | category | flops | bytes accessed | tf_op | source)
XLA Modules:
  0.0 68.6 jit_solution(9345950190689367674)
XLA Ops:
  0.6 66.5 %layer.1 = (bf16[32,512]{1,0:T(8,128)(2,1)}, bf16[32,64]{1,0:T(8,128)(2,1)}, bf16[32,64]{1,0:T(8,128)(2,1)}, f32[8,32]{1,0:T(8,128)}) custom-call(bf16[32,2048]{1,0:T(8,128)(2,1)} %refs_0_.1, f32[1,2048]{1,0:T(1,128)} %bitcast.13, bf16[32,512]{1,0:T(8,128)(2,1)} %refs_2_.1, bf16[32,64]{1,0:T(8,128)(2,1)} %refs_3_.1, bf16[32,64]{1,0:T(8,128)(2,1)} %refs_4_.1, ...), custom_call_target="tpu_custom_call" | custom-call | tf_op jit(solution)/shard_map/layer/pallas_call | solution.py:516
  67.2 1.4 %write.1 = (bf16[32,512]{1,0:T(8,128)(2,1)}, bf16[32,64]{1,0:T(8,128)(2,1)}, bf16[32,64]{1,0:T(8,128)(2,1)}, f32[8,32]{1,0:T(8,128)}) custom-call(bf16[32,512]{1,0:T(8,128)(2,1)} %get-tuple-element.12.refs_0_, bf16[32,64]{1,0:T(8,128)(2,1)} %get-tuple-element.13.refs_1_, bf16[32,64]{1,0:T(8,128)(2,1)} %get-tuple-element.14.refs_2_, ...), custom_call_target="tpu_custom_call" | custom-call | tf_op jit(solution)/shard_map/write/pallas_call | solution.py:579
